TPU v7x, 512 devices: a whole 4x4x16 slice. The times are simulated.
512 devices in a mesh: kv: 64 (over z, y), tp: 8 (over x, core).
Axes of the slice: x: 4, y: 4, z: 16, core: 2. Of those that a mesh axis runs over, the one named last changes fastest.
Arguments:
- tokens: bfloat16 [1024, 2048], P('kv', 'tp'), may hold values from -20 to 20
- attn_gain: bfloat16 [2048], replicated, may hold values from 0.099609375 to 1.8984375
- query_weight: bfloat16 [2048, 1024], P(None, 'tp'), may hold values from -0.125 to 0.125
- key_weight: bfloat16 [2048, 1024], P(None, 'tp'), may hold values from -0.125 to 0.125
- value_weight: bfloat16 [2048, 1024], P(None, 'tp'), may hold values from -0.125 to 0.125
- outgate_weight: bfloat16 [2048, 1024], P(None, 'tp'), may hold values from -0.125 to 0.125
- gate_weight: bfloat16 [2, 8, 2048], replicated, may hold values from -0.125 to 0.125
- forget_bias: float32 [8], replicated, may hold values from -1 to 4
- state_matrix: float32 [1024, 8, 128, 128], P('kv', 'tp'), may hold values from -1.8 to 1.8
- state_norm: float32 [1024, 8, 128], P('kv', 'tp'), may hold values from -1.8 to 1.8
- state_max: float32 [1024, 8], P('kv', 'tp'), may hold values from -1 to 1
- out_weight: bfloat16 [1024, 2048], P(None, 'tp'), may hold values from -0.1875 to 0.1875
- mlp_gain: bfloat16 [2048], P('tp'), may hold values from 0.099609375 to 1.8984375
- up_weight: bfloat16 [2048, 8192], P('tp', 'kv'), may hold values from -0.125 to 0.125
- down_weight: bfloat16 [8192, 2048], P('kv', 'tp'), may hold values from -0.0625 to 0.0625
Outputs:
- result: bfloat16 [1024, 2048], P('kv', 'tp')
- next_matrix: float32 [1024, 8, 128, 128], P('kv', 'tp')
- next_norm: float32 [1024, 8, 128], P('kv', 'tp')
- next_max: float32 [1024, 8], P('kv', 'tp')
All inputs are finite; a program needn't handle non-finite values.
Results may differ from a plain program's by a relative error of at most 0.013.
Values may be sent and summed in bfloat16 or wider, within the bound.
No kernel may reach another device: no remote copies, remote signals or barrier semaphores. Data moves between devices by JAX's collectives and lax.ppermute only.
A program may use at most 64 MiB of HBM per device.

v0:
```python
import jax
import jax.numpy as jnp
from jax import lax
from jax.sharding import Mesh
from jax.sharding import PartitionSpec as P

KV = ("kv_0", "kv_1")


epsilon = 1e-06


def from_everyone(array, axis):
    size = lax.axis_size(axis)
    return lax.all_to_all(
        jnp.broadcast_to(array[None], (size, *array.shape)), axis, 0, 0, tiled=True
    )


def laid_out(tiles, dim):
    tiles = jnp.moveaxis(tiles, 0, dim)
    shape = tiles.shape
    return tiles.reshape(*shape[:dim], shape[dim] * shape[dim + 1], *shape[dim + 2 :])


def gather_directly(array, axis, dim):
    tiles = from_everyone(array, axis)
    return laid_out(tiles, dim)


def whole_of(array, axes, dim):
    for axis in reversed(axes):
        array = lax.all_gather(array, axis, axis=dim, tiled=True)
    return array


def taken_together(array, axis):
    everything = from_everyone(array, axis)
    return jnp.sum(everything, axis=0)


def of_everyone(array, axis):
    everything = from_everyone(array, axis)
    return jnp.sum(everything.astype(jnp.float32), axis=0)


def cut_along(array, dim, size):
    shape = array.shape
    tiles = array.reshape(*shape[:dim], size, shape[dim] // size, *shape[dim + 1 :])
    return jnp.moveaxis(tiles, dim, 0)


def sent_and_summed(array, axis, dim):
    size = lax.axis_size(axis)
    tiles = lax.all_to_all(cut_along(array, dim, size), axis, 0, 0, tiled=True)
    return jnp.sum(tiles, axis=0)


def body(
    tokens,
    attn_gain,
    query_weight,
    key_weight,
    value_weight,
    outgate_weight,
    gate_weight,
    forget_bias,
    state_matrix,
    state_norm,
    state_max,
    out_weight,
    mlp_gain,
    up_weight,
    down_weight,
):
    sequences = tokens.shape[0]
    local_heads = state_matrix.shape[1]
    head_dim = state_matrix.shape[2]
    width = query_weight.shape[1]
    model_width = attn_gain.shape[0]
    first_head = lax.axis_index("tp") * local_heads
    my_gates = lax.dynamic_slice_in_dim(gate_weight, first_head, local_heads, 1).reshape(
        2 * local_heads, model_width
    )
    my_bias = lax.dynamic_slice_in_dim(forget_bias, first_head, local_heads, 0)
    gain_full = attn_gain.astype(jnp.float32)
    seg_values = gather_directly(tokens, "tp", 1).astype(jnp.float32)
    scaled = (seg_values * gain_full).astype(jnp.bfloat16)

    def product(weight):
        return jnp.dot(scaled, weight, preferred_element_type=jnp.float32)

    gate_part = jnp.einsum("sd,gd->sg", scaled, my_gates, preferred_element_type=jnp.float32)
    squares = jnp.sum(seg_values * seg_values, axis=1)
    query_acc = product(query_weight)
    key_acc = product(key_weight)
    value_acc = product(value_weight)
    outgate_acc = product(outgate_weight)
    scale_in = lax.rsqrt(squares / model_width + epsilon)[:, None]
    query_rows = (query_acc * scale_in).reshape(sequences, local_heads, head_dim)
    key_rows = (key_acc * scale_in * head_dim ** (-0.5)).reshape(sequences, local_heads, head_dim)
    value_rows = (value_acc * scale_in).reshape(sequences, local_heads, head_dim)
    outgate = (outgate_acc * scale_in).reshape(sequences, local_heads, head_dim)
    gate_pre = gate_part * scale_in
    in_gate = gate_pre[:, :local_heads]
    forget_log = jax.nn.log_sigmoid(gate_pre[:, local_heads:] + my_bias)
    next_max = jnp.maximum(forget_log + state_max, in_gate)
    kept_share = jnp.exp(forget_log + state_max - next_max)
    admitted = jnp.exp(in_gate - next_max)
    next_matrix = (
        kept_share[:, :, None, None] * state_matrix
        + admitted[:, :, None, None] * key_rows[:, :, :, None] * value_rows[:, :, None, :]
    )
    next_norm = kept_share[:, :, None] * state_norm + admitted[:, :, None] * key_rows
    numerator = jnp.einsum(
        "shd,shde->she", query_rows, next_matrix, precision=lax.Precision.HIGHEST
    )
    denominator = jnp.sum(query_rows * next_norm, axis=2)
    head_out = numerator / jnp.maximum(jnp.abs(denominator), 1.0)[:, :, None]
    mixed = (head_out * jax.nn.sigmoid(outgate)).reshape(sequences, width).astype(jnp.bfloat16)
    attended = jnp.dot(
        gather_directly(mixed, "tp", 1), out_weight, preferred_element_type=jnp.float32
    )
    residual = (tokens.astype(jnp.float32) + attended).astype(jnp.bfloat16)
    gain_mid = mlp_gain.astype(jnp.float32)
    rows_all = whole_of(residual, KV, 0)
    row_values = rows_all.astype(jnp.float32)
    row_squares = jnp.sum(row_values * row_values, axis=1)
    scaled_mid = (row_values * gain_mid).astype(jnp.bfloat16)
    partial_value = jnp.dot(scaled_mid, up_weight, preferred_element_type=jnp.float32)
    total_squares = taken_together(row_squares, "tp")
    row_scale = lax.rsqrt(total_squares / model_width + epsilon)
    up_value = of_everyone((partial_value * row_scale[:, None]).astype(jnp.bfloat16), "tp").astype(
        jnp.float32
    )
    hidden = jnp.square(jax.nn.relu(up_value)).astype(jnp.bfloat16)
    mixer_out = sent_and_summed(
        jnp.dot(hidden, down_weight, preferred_element_type=jnp.float32), KV, 0
    )
    result = (residual.astype(jnp.float32) + mixer_out).astype(jnp.bfloat16)
    return (result, next_matrix, next_norm, next_max)


def solution(mesh):
    split = Mesh(mesh.devices.reshape(16, 4, mesh.shape["tp"]), ("kv_0", "kv_1", "tp"))
    placed = (
        P(KV, "tp"),
        P(),
        P(None, "tp"),
        P(None, "tp"),
        P(None, "tp"),
        P(None, "tp"),
        P(),
        P(),
        P(KV, "tp", None, None),
        P(KV, "tp", None),
        P(KV, "tp"),
        P(None, "tp"),
        P("tp"),
        P("tp", KV),
        P(KV, "tp"),
    )
    return jax.shard_map(
        body,
        mesh=split,
        in_specs=placed,
        out_specs=(P(KV, "tp"), P(KV, "tp", None, None), P(KV, "tp", None), P(KV, "tp")),
        check_vma=False,
    )
```

profile of v0, /device:TPU:8, one launch (start us, length us, event | category | flops | bytes accessed | tf_op | source)
XLA Modules:
  0.0 183.4 jit_solution(13967047711854969960)
XLA Ops:
  0.6 0.0 copy-start
  0.6 0.0 copy-start.9
  0.7 0.0 copy-start.2
  0.7 1.4 broadcast_in_dim.8
  2.1 4.3 %all-to-all-start = ((bf16[8,16,256]{2,1,0:T(8,128)(2,1)}), bf16[8,16,256]{2,1,0:T(8,128)(2,1)S(1)}, u32[]{:S(2)}, u32[]{:S(2)}) async-start(bf16[8,16,256]{2,1,0:T(8,128)(2,1)} %broadcast_in_dim.8), calls=%async_computation | async-start | bytes 131072 | tf_op jit(solution)/shard_map/all_to_all | solution.py:15
  6.4 0.9 constant_dynamic-slice_fusion
  7.3 0.7 mul.149
  8.0 0.7 convert_element_type.67
  8.7 1.2 dynamic_slice.7
  9.9 2.1 %all-to-all-done = bf16[8,16,256]{2,1,0:T(8,128)(2,1)S(1)} async-done(((bf16[8,16,256]{2,1,0:T(8,128)(2,1)}), bf16[8,16,256]{2,1,0:T(8,128)(2,1)S(1)}, u32[]{:S(2)}, u32[]{:S(2)}) %all-to-all-start) | async-done | bytes 65568 | tf_op jit(solution)/shard_map/all_to_all | solution.py:15
  12.0 0.1 fusion.19
  12.2 0.1 convolution_multiply_fusion.5
  12.3 1.3 exponential_bitcast_fusion
  13.7 0.0 copy-start.6
  13.7 1.2 convolution_multiply_fusion.2
  15.0 0.0 copy-start.7
  15.0 1.3 fusion.7
  16.2 0.0 copy-done
  16.3 0.0 copy-done.9
  16.3 0.8 fusion.24
  17.1 0.0 copy-start.3
  17.1 0.0 copy-start.5
  17.1 0.0 copy-done.2
  17.2 0.4 multiply_add_fusion
  17.5 0.0 copy-done.6
  17.6 0.0 copy-start.1
  17.6 0.0 copy-start.10
  17.6 0.0 copy-start.8
  17.6 1.0 fusion.11
  18.6 0.0 copy-done.7
  18.6 0.2 fusion.8
  18.8 7.9 %all_to_all.26 = bf16[8,16,128]{2,1,0:T(8,128)(2,1)S(1)} all-to-all(bf16[8,16,128]{2,1,0:T(8,128)(2,1)S(1)} %broadcast_in_dim.9), channel_id=1, replica_groups=mesh['kv_0'=16,'kv_1'=4,'tp'=8] {'tp'}, dimensions={0} | all-to-all | bytes 65536 | tf_op jit(solution)/shard_map/all_to_all | solution.py:15
  26.7 0.0 copy-done.3
  26.7 0.0 copy-done.5
  26.7 0.2 fusion.1
  26.9 13.5 %all_gather.6 = bf16[64,256]{1,0:T(8,128)(2,1)S(1)} all-gather(bf16[16,256]{1,0:T(8,128)(2,1)S(1)} %fusion.1), channel_id=1, replica_groups=mesh['kv_0'=16,'kv_1'=4,'tp'=8] {'kv_1'}, dimensions={0}, use_global_device_ids=true | all-gather | bytes 40960 | tf_op jit(solution)/shard_map/all_gather | solution.py:33
  40.4 36.9 %all_gather.7 = bf16[1024,256]{1,0:T(8,128)(2,1)S(1)} all-gather(bf16[64,256]{1,0:T(8,128)(2,1)S(1)} %all_gather.6), channel_id=1, replica_groups=mesh['kv_0'=16,'kv_1'=4,'tp'=8] {'kv_0'}, dimensions={0}, use_global_device_ids=true | all-gather | bytes 557056 | tf_op jit(solution)/shard_map/all_gather | solution.py:33
  77.2 0.2 fusion.10
  77.5 0.6 broadcast_in_dim.10
  78.1 3.3 %all-to-all-start.2 = ((f32[8,1,1024]{2,1,0:T(1,128)}), f32[8,1,1024]{2,1,0:T(1,128)S(1)}, u32[]{:S(2)}, u32[]{:S(2)}) async-start(f32[8,1,1024]{2,1,0:T(1,128)} %broadcast_in_dim.10), calls=%async_computation.2 | async-start | bytes 65536 | tf_op jit(solution)/shard_map/all_to_all | solution.py:15
  81.4 0.0 copy-done.10
  81.4 5.3 %all-to-all-done.2 = f32[8,1,1024]{2,1,0:T(1,128)S(1)} async-done(((f32[8,1,1024]{2,1,0:T(1,128)}), f32[8,1,1024]{2,1,0:T(1,128)S(1)}, u32[]{:S(2)}, u32[]{:S(2)}) %all-to-all-start.2) | async-done | bytes 32800 | tf_op jit(solution)/shard_map/all_to_all | solution.py:15
  86.8 0.0 copy-done.8
  86.8 0.3 fusion
  87.2 0.0 copy-done.1
  87.2 0.3 broadcast_in_dim.11
  87.5 29.7 %all_to_all.27 = bf16[8,1024,128]{2,1,0:T(8,128)(2,1)S(1)} all-to-all(bf16[8,1024,128]{2,1,0:T(8,128)(2,1)S(1)} %broadcast_in_dim.11), channel_id=1, replica_groups=mesh['kv_0'=16,'kv_1'=4,'tp'=8] {'tp'}, dimensions={0} | all-to-all | bytes 4194304 | tf_op jit(solution)/shard_map/all_to_all | solution.py:15
  117.1 0.0 copy-start.4
  117.1 0.3 convert_reduce_fusion
  117.4 0.5 copy-done.4
  118.0 0.3 fusion.15
  118.2 64.5 %all_to_all.28 = f32[64,16,256]{2,1,0:T(8,128)S(1)} all-to-all(f32[64,16,256]{2,1,0:T(8,128)S(1)} %bitcast.55), channel_id=1, replica_groups=mesh['kv_0'=16,'kv_1'=4,'tp'=8] {'kv_0','kv_1'}, dimensions={0} | all-to-all | bytes 2097152 | tf_op jit(solution)/shard_map/all_to_all | solution.py:55
  182.7 0.1 reduce_sum.59
  182.8 0.6 add_convert_fusion
  (11 shorter events, 0.1 us)
Async XLA Ops:
  0.6 15.6 %copy-start = (bf16[2048,128]{1,0:T(8,128)(2,1)S(1)}, bf16[2048,128]{1,0:T(8,128)(2,1)}, u32[]{:S(2)}) copy-start(bf16[2048,128]{1,0:T(8,128)(2,1)} %param.17) | copy-start | bytes 1572868
  0.6 15.6 %copy-start.9 = (f32[16,1,128]{2,1,0:T(1,128)S(1)}, f32[16,1,128]{2,1,0:T(1,128)}, u32[]{:S(2)}) copy-start(f32[16,1,128]{2,1,0:T(1,128)} %param.24) | copy-start | bytes 24580
  0.7 16.5 %copy-start.2 = (f32[16,1,128,128]{3,2,1,0:T(8,128)S(1)}, f32[16,1,128,128]{3,2,1,0:T(8,128)}, u32[]{:S(2)}) copy-start(f32[16,1,128,128]{3,2,1,0:T(8,128)} %param.23) | copy-start | bytes 3145732
  2.1 9.9 %all-to-all-start = ((bf16[8,16,256]{2,1,0:T(8,128)(2,1)}), bf16[8,16,256]{2,1,0:T(8,128)(2,1)S(1)}, u32[]{:S(2)}, u32[]{:S(2)}) async-start(bf16[8,16,256]{2,1,0:T(8,128)(2,1)} %broadcast_in_dim.8), calls=%async_computation | async-start | bytes 131072 | tf_op jit(solution)/shard_map/all_to_all | solution.py:15
  13.7 3.9 %copy-start.6 = (f32[16,1]{0,1:T(1,128)}, f32[16,1]{0,1:T(1,128)S(1)}, u32[]{:S(2)}) copy-start(f32[16,1]{0,1:T(1,128)S(1)} %get-tuple-element.27) | copy-start | bytes 196
  15.0 3.6 %copy-start.7 = (bf16[2048,128]{1,0:T(8,128)(2,1)S(1)}, bf16[2048,128]{1,0:T(8,128)(2,1)}, u32[]{:S(2)}) copy-start(bf16[2048,128]{1,0:T(8,128)(2,1)} %param.20) | copy-start | bytes 1572868
  17.1 9.6 %copy-start.3 = (bf16[1024,256]{1,0:T(8,128)(2,1)S(1)}, bf16[1024,256]{1,0:T(8,128)(2,1)}, u32[]{:S(2)}) copy-start(bf16[1024,256]{1,0:T(8,128)(2,1)} %param.26) | copy-start | bytes 1572868
  17.1 9.6 %copy-start.5 = (bf16[16,256]{1,0:T(8,128)(2,1)S(1)}, bf16[16,256]{1,0:T(8,128)(2,1)}, u32[]{:S(2)}) copy-start(bf16[16,256]{1,0:T(8,128)(2,1)} %param.15) | copy-start | bytes 24580
  17.6 69.6 %copy-start.1 = (f32[16,1,128,128]{3,2,1,0:T(8,128)}, f32[16,1,128,128]{3,2,1,0:T(8,128)S(1)}, u32[]{:S(2)}) copy-start(f32[16,1,128,128]{3,2,1,0:T(8,128)S(1)} %multiply_add_fusion) | copy-start | bytes 3145732
  17.6 63.9 %copy-start.10 = (bf16[256]{0:T(256)(128)(2,1)S(1)}, bf16[256]{0:T(256)(128)(2,1)}, u32[]{:S(2)}) copy-start(bf16[256]{0:T(256)(128)(2,1)} %param.27) | copy-start | bytes 1540
  17.6 69.3 %copy-start.8 = (bf16[256,128]{1,0:T(8,128)(2,1)S(1)}, bf16[256,128]{1,0:T(8,128)(2,1)}, u32[]{:S(2)}) copy-start(bf16[256,128]{1,0:T(8,128)(2,1)} %param.28) | copy-start | bytes 196612
  78.1 8.7 %all-to-all-start.2 = ((f32[8,1,1024]{2,1,0:T(1,128)}), f32[8,1,1024]{2,1,0:T(1,128)S(1)}, u32[]{:S(2)}, u32[]{:S(2)}) async-start(f32[8,1,1024]{2,1,0:T(1,128)} %broadcast_in_dim.10), calls=%async_computation.2 | async-start | bytes 65536 | tf_op jit(solution)/shard_map/all_to_all | solution.py:15
  117.1 0.8 copy-start.4
where the time goes:
time: 184 us; the launch traced here: 183 us
  blocking collectives  152 us (83%)
  starting transfers between devices  7.62 us (4%)
  waiting for transfers between devices  7.48 us (4%)
  local copies, waits for them, and re-layouts  5.75 us (3%)
  matrix products  5.43 us (3%)
  other arithmetic  3.83 us (2%)
    all_to_all x1, blocking collectives, sent_and_summed(): tiles = lax.all_to_all(cut_along(array, dim, size), axis, 0, 0, tiled=True)  64.5 us
    all_gather x2, blocking collectives, whole_of(): array = lax.all_gather(array, axis, axis=dim, tiled=True)  50.4 us
    all_to_all x2, blocking collectives, from_everyone(): lax.all_to_all(jnp.broadcast_to(array[None], (size, *array.shape)), axis,...  37.6 us
    all_to_all x2, starting transfers between devices, from_everyone(): lax.all_to_all(jnp.broadcast_to(array[None], (size, *array.shape)), axis,...  7.62 us
    all_to_all x2, waiting for transfers between devices, from_everyone(): lax.all_to_all(jnp.broadcast_to(array[None], (size, *array.shape)), axis,...  7.48 us
  transfers between devices with their start and end apart: 2, of which 2 were waited for; matrix products, arithmetic and copies ran while one was open for 2% of the time, Pallas kernels for 0%

commit v1 on v0

v1 whole, which is shorter than its diff:
```python
import jax
import jax.numpy as jnp
from jax import lax
from jax.sharding import Mesh
from jax.sharding import PartitionSpec as P

KV = ("z", "y")
TP = ("x", "c")
NEAR = ("z", "c")
epsilon = 1e-06
f32 = jnp.float32
bf16 = jnp.bfloat16


def axis_total(axes):
    axes = axes if isinstance(axes, tuple) else (axes,)
    total = 1
    for name in axes:
        total *= lax.axis_size(name)
    return total


def from_everyone(array, axes):
    return lax.all_to_all(
        jnp.broadcast_to(array[None], (axis_total(axes), *array.shape)), axes, 0, 0, tiled=True
    )


def shifted(array, axis, step):
    size = lax.axis_size(axis)
    return lax.ppermute(array, axis, [(i, (i + step) % size) for i in range(size)])


def gather_columns(array, axes):
    tiles = from_everyone(array, axes)
    count, rows, columns = tiles.shape
    return jnp.moveaxis(tiles, 0, 1).reshape(rows, count * columns)


def body(
    tokens,
    attn_gain,
    query_weight,
    key_weight,
    value_weight,
    outgate_weight,
    gate_weight,
    forget_bias,
    state_matrix,
    state_norm,
    state_max,
    out_weight,
    mlp_gain,
    up_weight,
    down_weight,
):
    sequences = tokens.shape[0]
    head_dim = state_matrix.shape[2]
    model_width = attn_gain.shape[0]
    head = lax.axis_index(TP)

    up_scaled = (up_weight.astype(f32) * mlp_gain.astype(f32)[:, None]).astype(bf16)
    block = jnp.stack([up_scaled, down_weight.T])
    following = shifted(block, "y", 1)
    preceding = shifted(block, "y", -1)
    opposite = shifted(following, "y", 1)
    mixer_own = jnp.stack([block, following, preceding, opposite], 1)
    up_other = shifted(mixer_own[0], "c", 1)
    down_other = shifted(mixer_own[1], "c", 1)
    up_parts = (mixer_own[0], up_other)
    down_parts = (mixer_own[1], down_other)

    gates = lax.dynamic_index_in_dim(gate_weight, head, 1, keepdims=False)
    my_bias = lax.dynamic_index_in_dim(forget_bias, head, 0, keepdims=True)
    values = gather_columns(tokens, TP).astype(f32)
    scaled = (values * attn_gain.astype(f32)).astype(bf16)

    def product(weight):
        return jnp.dot(scaled, weight, preferred_element_type=f32)

    gate_part = jnp.einsum("sd,gd->sg", scaled, gates, preferred_element_type=f32)
    squares = jnp.sum(values * values, axis=1)
    scale_in = lax.rsqrt(squares / model_width + epsilon)[:, None]
    query = product(query_weight) * scale_in
    key = product(key_weight) * scale_in * head_dim ** (-0.5)
    value = product(value_weight) * scale_in
    outgate = product(outgate_weight) * scale_in
    gate_pre = gate_part * scale_in
    in_gate = gate_pre[:, :1]
    forget_log = jax.nn.log_sigmoid(gate_pre[:, 1:] + my_bias)
    next_max = jnp.maximum(forget_log + state_max, in_gate)
    kept = jnp.exp(forget_log + state_max - next_max)
    admitted = jnp.exp(in_gate - next_max)
    next_matrix = (
        kept[:, :, None] * state_matrix[:, 0]
        + (admitted * key)[:, :, None] * value[:, None, :]
    )
    next_norm = kept * state_norm[:, 0] + admitted * key
    numerator = jnp.sum(query[:, :, None] * next_matrix, axis=1)
    denominator = jnp.sum(query * next_norm, axis=1, keepdims=True)
    head_out = numerator / jnp.maximum(jnp.abs(denominator), 1.0)
    mixed = (head_out * jax.nn.sigmoid(outgate)).astype(bf16)
    mixed_full = gather_columns(mixed, TP)
    attended = jnp.dot(mixed_full, out_weight, preferred_element_type=f32)
    residual = (tokens.astype(f32) + attended).astype(bf16)

    cores = lax.axis_size("c")
    near = lax.axis_size("z")
    share = sequences // cores
    columns = residual.shape[1]
    outgoing = jnp.broadcast_to(
        residual.reshape(1, cores, share, columns), (near, cores, share, columns)
    ).reshape(near * cores, share, columns)
    rows = lax.all_to_all(outgoing, NEAR, 0, 0, tiled=True)
    rows = rows.reshape(near, cores, share, columns)
    core = lax.axis_index("c")
    rows = [
        lax.dynamic_index_in_dim(rows, index, 1, keepdims=False).reshape(near * share, columns)
        for index in (core, 1 - core)
    ]
    partial = sum(
        jnp.einsum("rf,zfh->rzh", mine, part, preferred_element_type=f32)
        for mine, part in zip(rows, up_parts)
    )
    partial = partial.reshape(near * share, -1)
    own = sum(jnp.sum(jnp.square(mine.astype(f32)), axis=1) for mine in rows)
    high = own.astype(bf16)
    low = (own - high.astype(f32)).astype(bf16)
    packed = jnp.concatenate(
        [partial.astype(bf16), jnp.pad(jnp.stack([high, low], 1), ((0, 0), (0, 126)))], axis=1
    )
    sums = from_everyone(packed, "x")
    gathered = jnp.sum(sums.astype(f32), axis=0)
    hidden_width = partial.shape[1]
    total = gathered[:, hidden_width : hidden_width + 1] + gathered[:, hidden_width + 1 : hidden_width + 2]
    scale_mid = lax.rsqrt(total / model_width + epsilon)
    hidden = jnp.square(jax.nn.relu(gathered[:, :hidden_width] * scale_mid)).astype(bf16)
    hidden = hidden.reshape(near * share, up_parts[0].shape[0], -1)
    down = [
        jnp.einsum("rzh,zfh->rf", hidden, part, preferred_element_type=f32)
        .astype(bf16)
        .reshape(near, share, columns)
        for part in down_parts
    ]
    first = core == 0
    down = [jnp.where(first, down[0], down[1]), jnp.where(first, down[1], down[0])]
    back = lax.all_to_all(
        jnp.stack(down, 1).reshape(near * cores, share, columns), NEAR, 0, 0, tiled=True
    )
    mixer_out = jnp.sum(back.reshape(near, cores, share, columns).astype(f32), axis=0)
    result = (residual.astype(f32) + mixer_out.reshape(sequences, columns)).astype(bf16)
    return (result, next_matrix[:, None], next_norm[:, None], next_max)


def solution(mesh):
    split = Mesh(
        mesh.devices.reshape(16, 4, 4, 2), ("z", "y", "x", "c")
    )
    placed = (
        P(KV, TP),
        P(),
        P(None, TP),
        P(None, TP),
        P(None, TP),
        P(None, TP),
        P(),
        P(),
        P(KV, TP, None, None),
        P(KV, TP, None),
        P(KV, TP),
        P(None, TP),
        P(TP),
        P(TP, KV),
        P(KV, TP),
    )
    return jax.shard_map(
        body,
        mesh=split,
        in_specs=placed,
        out_specs=(P(KV, TP), P(KV, TP, None, None), P(KV, TP, None), P(KV, TP)),
        check_vma=False,
    )
```

time: 184 us -> 108 us (0.59)
  the two profiles are of different devices: /device:TPU:8 before, /device:TPU:1 now
where the time goes in v1:
time: 108 us; the launch traced here: 107 us
  starting transfers between devices  58.5 us (54%)
  waiting for transfers between devices  30.7 us (28%)
  local copies, waits for them, and re-layouts  7.76 us (7%)
  other arithmetic  6.74 us (6%)
  matrix products  2.6 us (2%)
  between operations  1.1 us (1%)
    all_to_all x3, starting transfers between devices, from_everyone(): lax.all_to_all(jnp.broadcast_to(array[None], (axis_total(axes), *array.sh...  18.5 us
    ppermute x5, starting transfers between devices, shifted(): lax.ppermute(array, axis, [(i, (i + step) % size) for i in range(size)])  14.7 us
    all_to_all x1, waiting for transfers between devices, body(): lax.all_to_all(jnp.stack(down, 1).reshape(near * cores, share, columns),...  14.5 us
    all_to_all x1, starting transfers between devices, body(): lax.all_to_all(jnp.stack(down, 1).reshape(near * cores, share, columns),...  13.7 us
    all_to_all x1, starting transfers between devices, body(): rows = lax.all_to_all(outgoing, NEAR, 0, 0, tiled=True)  11.7 us
    all_to_all x3, waiting for transfers between devices, from_everyone(): lax.all_to_all(jnp.broadcast_to(array[None], (axis_total(axes), *array.sh...  9.75 us
    ppermute x5, waiting for transfers between devices, shifted(): lax.ppermute(array, axis, [(i, (i + step) % size) for i in range(size)])  6.29 us
    broadcast_in_dim x3, local copies, waits for them, and re-layouts, from_everyone(): jnp.broadcast_to(array[None], (axis_total(axes), *array.shape))  2.93 us
  transfers between devices with their start and end apart: 10, of which 7 were waited for; matrix products, arithmetic and copies ran while one was open for 8% of the time, Pallas kernels for 0%

profile of v1, /device:TPU:1, one launch (start us, length us, event | category | flops | bytes accessed | tf_op | source)
XLA Modules:
  0.0 107.4 jit_solution(8220453348695489123)
XLA Ops:
  0.6 0.0 copy-start
  0.7 1.4 %broadcast_in_dim.12 = bf16[8,16,256]{2,1,0:T(8,128)(2,1)} broadcast(bf16[16,256]{1,0:T(8,128)(2,1)} %param.15), dimensions={1,2} | broadcast | bytes 73728 | tf_op jit(solution)/shard_map/broadcast_in_dim | solution.py:25
  2.1 10.2 %all-to-all-start = ((bf16[8,16,256]{2,1,0:T(8,128)(2,1)}), bf16[8,16,256]{2,1,0:T(8,128)(2,1)S(1)}, u32[]{:S(2)}, u32[]{:S(2)}) async-start(bf16[8,16,256]{2,1,0:T(8,128)(2,1)} %broadcast_in_dim.12), calls=%async_computation | async-start | bytes 131072 | tf_op jit(solution)/shard_map/all_to_all | solution.py:24
  12.3 0.7 convert_element_type.134
  13.0 0.9 copy.74
  13.9 0.9 constant_dynamic-slice_fusion
  14.8 0.7 mul.165
  15.5 0.7 convert_element_type.124
  16.2 1.2 %dynamic_slice.16 = f32[1]{0:T(128)} dynamic-slice(f32[8]{0:T(128)} %param.22, s32[]{:T(128)S(6)} %select_n.50), dynamic_slice_sizes={1} | dynamic-slice | bytes 12 | tf_op jit(solution)/shard_map/jit(dynamic_index_in_dim)/dynamic_slice | solution.py:74
  17.4 0.0 all-to-all-done
  17.4 0.1 fusion.24
  17.6 0.1 convolution_multiply_fusion.4
  17.7 1.3 %exponential_bitcast_fusion = (f32[16]{0:T(128)S(1)}, f32[16,1]{0,1:T(1,128)S(1)}) fusion(f32[16,2]{0,1:T(2,128)S(1)} %convolution_multiply_fusion.4, f32[16,1]{0,1:T(1,128)} %param.25, f32[]{:T(128)} %bitcast.2), kind=kLoop, calls=%fused_computation.85 | loop fusion | flops 192 | bytes 324 | tf_op jit(solution)/shard_map/mul | solution.py:95
  19.1 0.0 copy-start.1
  19.2 0.2 convolution_multiply_fusion.1
  19.3 0.0 copy-done.11
  19.3 0.0 copy-start.12
  19.4 0.2 fusion.8
  19.5 0.0 copy-start.5
  19.6 0.0 copy-done.10
  19.6 0.0 copy-done
  19.6 0.8 multiply_reduce_fusion.2
  20.5 0.0 copy-start.3
  20.5 0.0 copy-start.7
  20.5 0.7 fusion.12
  21.2 0.2 fusion.9
  21.4 0.0 copy-done.5
  21.5 0.6 broadcast_in_dim.13
  22.1 4.8 %all-to-all-start.1 = ((bf16[8,16,128]{2,1,0:T(8,128)(2,1)}), bf16[8,16,128]{2,1,0:T(8,128)(2,1)S(1)}, u32[]{:S(2)}, u32[]{:S(2)}) async-start(bf16[8,16,128]{2,1,0:T(8,128)(2,1)} %broadcast_in_dim.13), calls=%async_computation.1 | async-start | bytes 65536 | tf_op jit(solution)/shard_map/all_to_all | solution.py:24
  26.9 1.9 %collective-permute-start = (bf16[2,256,128]{1,2,0:T(8,128)(2,1)S(1)}, bf16[2,256,128]{1,2,0:T(8,128)(2,1)S(1)}, u32[]{:S(2)}, u32[]{:S(2)}) collective-permute-start(bf16[2,256,128]{1,2,0:T(8,128)(2,1)S(1)} %get-tuple-element.36), channel_id=1, source_target_pairs={{0,8},{8,16},{16,24},{24,0},{1,9},{9,17},{17,25},{25,1},{2,10},{10... | collective-permute-start | bytes 393224 | tf_op jit(solution)/shard_map/ppermute | solution.py:31
  28.8 2.8 %all-to-all-done.1 = bf16[8,16,128]{2,1,0:T(8,128)(2,1)S(1)} async-done(((bf16[8,16,128]{2,1,0:T(8,128)(2,1)}), bf16[8,16,128]{2,1,0:T(8,128)(2,1)S(1)}, u32[]{:S(2)}, u32[]{:S(2)}) %all-to-all-start.1) | async-done | bytes 32800 | tf_op jit(solution)/shard_map/all_to_all | solution.py:24
  31.6 0.2 fusion.2
  31.8 0.7 broadcast_in_dim.15
  32.5 11.7 %all-to-all-start.2 = ((bf16[32,8,256]{2,1,0:T(8,128)(2,1)}), bf16[32,8,256]{2,1,0:T(8,128)(2,1)S(1)}, u32[]{:S(2)}, u32[]{:S(2)}) async-start(bf16[32,8,256]{2,1,0:T(8,128)(2,1)} %bitcast.9), calls=%async_computation.2 | async-start | bytes 262144 | tf_op jit(solution)/shard_map/all_to_all | solution.py:114
  44.1 4.6 %collective-permute-start.1 = (bf16[2,256,128]{1,2,0:T(8,128)(2,1)S(1)}, bf16[2,256,128]{1,2,0:T(8,128)(2,1)S(1)}, u32[]{:S(2)}, u32[]{:S(2)}) collective-permute-start(bf16[2,256,128]{1,2,0:T(8,128)(2,1)S(1)} %get-tuple-element.36), channel_id=1, source_target_pairs={{0,24},{8,0},{16,8},{24,16},{1,25},{9,1},{17,9},{25,17},{2,26},{10... | collective-permute-start | bytes 393224 | tf_op jit(solution)/shard_map/ppermute | solution.py:31
  48.8 0.0 collective-permute-done
  48.8 1.9 %collective-permute-start.2 = (bf16[2,256,128]{1,2,0:T(8,128)(2,1)S(1)}, bf16[2,256,128]{1,2,0:T(8,128)(2,1)S(1)}, u32[]{:S(2)}, u32[]{:S(2)}) collective-permute-start(bf16[2,256,128]{1,2,0:T(8,128)(2,1)S(1)} %collective-permute-done), channel_id=1, source_target_pairs={{0,8},{8,16},{16,24},{24,0},{1,9},{9,17},{17,25},{25,1},{2,10},{10... | collective-permute-start | bytes 393224 | tf_op jit(solution)/shard_map/ppermute | solution.py:31
  50.7 0.7 collective-permute-done.1
  51.4 5.1 %collective-permute-done.2 = bf16[2,256,128]{1,2,0:T(8,128)(2,1)S(1)} collective-permute-done((bf16[2,256,128]{1,2,0:T(8,128)(2,1)S(1)}, bf16[2,256,128]{1,2,0:T(8,128)(2,1)S(1)}, u32[]{:S(2)}, u32[]{:S(2)}) %collective-permute-start.2) | collective-permute-done | bytes 131104 | tf_op jit(solution)/shard_map/ppermute | solution.py:31
  56.4 0.1 pad_maximum_fusion
  56.5 0.1 slice_bitcast_fusion.2
  56.6 3.3 %collective-permute-start.3 = (bf16[4,256,128]{1,2,0:T(8,128)(2,1)S(1)}, bf16[4,256,128]{1,2,0:T(8,128)(2,1)S(1)}, u32[]{:S(2)}, u32[]{:S(2)}) collective-permute-start(bf16[4,256,128]{1,2,0:T(8,128)(2,1)S(1)} %get-tuple-element.30), channel_id=1, source_target_pairs={{0,1},{1,0},{2,3},{3,2},{4,5},{5,4},{6,7},{7,6},{8,9},{9,8},{10,11... | collective-permute-start | bytes 786440 | tf_op jit(solution)/shard_map/ppermute | solution.py:31
  59.9 0.1 all-to-all-done.2
  60.0 0.1 multiply_reduce_fusion
  60.1 0.1 add.108
  60.2 0.2 fusion.33
  60.4 0.6 collective-permute-done.3
  61.0 0.2 fusion.31
  61.3 0.2 copy.78
  61.5 0.9 broadcast_in_dim.16
  62.4 3.5 %all-to-all-start.3 = ((bf16[4,128,640]{2,1,0:T(8,128)(2,1)}), bf16[4,128,640]{2,1,0:T(8,128)(2,1)S(1)}, u32[]{:S(2)}, u32[]{:S(2)}) async-start(bf16[4,128,640]{2,1,0:T(8,128)(2,1)} %broadcast_in_dim.16), calls=%async_computation.3 | async-start | bytes 1310720 | tf_op jit(solution)/shard_map/all_to_all | solution.py:24
  65.9 2.9 %collective-permute-start.4 = (bf16[4,256,128]{1,2,0:T(8,128)(2,1)S(1)}, bf16[4,256,128]{1,2,0:T(8,128)(2,1)S(1)}, u32[]{:S(2)}, u32[]{:S(2)}) collective-permute-start(bf16[4,256,128]{1,2,0:T(8,128)(2,1)S(1)} %get-tuple-element.31), channel_id=1, source_target_pairs={{0,1},{1,0},{2,3},{3,2},{4,5},{5,4},{6,7},{7,6},{8,9},{9,8},{10,11... | collective-permute-start | bytes 786440 | tf_op jit(solution)/shard_map/ppermute | solution.py:31
  68.8 7.0 %all-to-all-done.3 = bf16[4,128,640]{2,1,0:T(8,128)(2,1)S(1)} async-done(((bf16[4,128,640]{2,1,0:T(8,128)(2,1)}), bf16[4,128,640]{2,1,0:T(8,128)(2,1)S(1)}, u32[]{:S(2)}, u32[]{:S(2)}) %all-to-all-start.3) | async-done | bytes 655392 | tf_op jit(solution)/shard_map/all_to_all | solution.py:24
  75.8 0.1 convert_reduce_fusion
  75.9 0.0 copy-start.6
  75.9 0.2 fusion.28
  76.1 0.0 collective-permute-done.4
  76.1 0.2 fusion.1
  76.3 0.2 select_bitcast_fusion.1
  76.6 0.7 pad_maximum_fusion.3
  77.2 13.7 %all-to-all-start.4 = ((bf16[32,8,256]{2,1,0:T(8,128)(2,1)}), bf16[32,8,256]{2,1,0:T(8,128)(2,1)S(1)}, u32[]{:S(2)}, u32[]{:S(2)}) async-start(bf16[32,8,256]{2,1,0:T(8,128)(2,1)} %bitcast.38), calls=%async_computation.4 | async-start | bytes 262144 | tf_op jit(solution)/shard_map/all_to_all | solution.py:147
  90.9 1.3 %multiply_add_fusion = f32[16,1,128,128]{3,2,1,0:T(8,128)} fusion(f32[16,1,128,128]{3,2,1,0:T(8,128)S(1)} %copy-done.1, f32[16,128]{1,0:T(8,128)S(1)} %convolution_multiply_fusion.1, f32[16,128]{1,0:T(8,128)S(1)} %copy-done.6, f32[16]{0:T(128)S(1)} %copy-done.9), kind=kLoop, calls=%fused_computation.23 | loop fusion | flops 786432 | bytes 2113600 | tf_op jit(solution)/shard_map/add | solution.py:95
  92.2 14.5 %all-to-all-done.4 = bf16[32,8,256]{2,1,0:T(8,128)(2,1)S(1)} async-done(((bf16[32,8,256]{2,1,0:T(8,128)(2,1)}), bf16[32,8,256]{2,1,0:T(8,128)(2,1)S(1)}, u32[]{:S(2)}, u32[]{:S(2)}) %all-to-all-start.4) | async-done | bytes 131104 | tf_op jit(solution)/shard_map/all_to_all | solution.py:147
  106.8 0.6 fusion.40
  (32 shorter events, 0.2 us)
Async XLA Ops:
  0.6 18.9 %copy-start = (bf16[2048,128]{1,0:T(8,128)(2,1)S(1)}, bf16[2048,128]{1,0:T(8,128)(2,1)}, u32[]{:S(2)}) copy-start(bf16[2048,128]{1,0:T(8,128)(2,1)} %param.17) | copy-start | bytes 1572868
  0.6 18.5 %copy-start.2 = (bf16[2048,128]{1,0:T(8,128)(2,1)S(1)}, bf16[2048,128]{1,0:T(8,128)(2,1)}, u32[]{:S(2)}) copy-start(bf16[2048,128]{1,0:T(8,128)(2,1)} %param.19) | copy-start | bytes 1572868
  2.1 17.3 %copy-start.11 = (bf16[2048,128]{1,0:T(8,128)(2,1)S(1)}, bf16[2048,128]{1,0:T(8,128)(2,1)}, u32[]{:S(2)}) copy-start(bf16[2048,128]{1,0:T(8,128)(2,1)} %param.18) | copy-start | bytes 1572868
  2.1 15.3 %all-to-all-start = ((bf16[8,16,256]{2,1,0:T(8,128)(2,1)}), bf16[8,16,256]{2,1,0:T(8,128)(2,1)S(1)}, u32[]{:S(2)}, u32[]{:S(2)}) async-start(bf16[8,16,256]{2,1,0:T(8,128)(2,1)} %broadcast_in_dim.12), calls=%async_computation | async-start | bytes 131072 | tf_op jit(solution)/shard_map/all_to_all | solution.py:24
  17.6 2.0 %copy-start.13 = (f32[16,1,128]{2,1,0:T(1,128)S(1)}, f32[16,1,128]{2,1,0:T(1,128)}, u32[]{:S(2)}) copy-start(f32[16,1,128]{2,1,0:T(1,128)} %param.24) | copy-start | bytes 24580
  19.0 0.5 copy-start.10
  19.1 1.4 %copy-start.8 = (f32[16]{0:T(128)}, f32[16]{0:T(128)S(1)}, u32[]{:S(2)}) copy-start(f32[16]{0:T(128)S(1)} %get-tuple-element.28) | copy-start | bytes 196
  19.1 1.3 %copy-start.1 = (f32[16,1,128,128]{3,2,1,0:T(8,128)S(1)}, f32[16,1,128,128]{3,2,1,0:T(8,128)}, u32[]{:S(2)}) copy-start(f32[16,1,128,128]{3,2,1,0:T(8,128)} %param.23) | copy-start | bytes 3145732
  19.3 1.9 %copy-start.12 = (bf16[2048,128]{1,0:T(8,128)(2,1)S(1)}, bf16[2048,128]{1,0:T(8,128)(2,1)}, u32[]{:S(2)}) copy-start(bf16[2048,128]{1,0:T(8,128)(2,1)} %param.20) | copy-start | bytes 1572868
  19.5 1.9 %copy-start.5 = (f32[16,128]{1,0:T(8,128)}, f32[16,128]{1,0:T(8,128)S(1)}, u32[]{:S(2)}) copy-start(f32[16,128]{1,0:T(8,128)S(1)} %fusion.8) | copy-start | bytes 24580
  20.4 6.5 %copy-start.4 = (bf16[128,256]{1,0:T(8,128)(2,1)S(1)}, bf16[128,256]{1,0:T(8,128)(2,1)}, u32[]{:S(2)}) copy-start(bf16[128,256]{1,0:T(8,128)(2,1)} %param.29) | copy-start | bytes 196612
  20.5 11.2 %copy-start.3 = (bf16[1024,256]{1,0:T(8,128)(2,1)S(1)}, bf16[1024,256]{1,0:T(8,128)(2,1)}, u32[]{:S(2)}) copy-start(bf16[1024,256]{1,0:T(8,128)(2,1)} %param.26) | copy-start | bytes 1572868
  20.5 11.1 %copy-start.7 = (bf16[16,256]{1,0:T(8,128)(2,1)S(1)}, bf16[16,256]{1,0:T(8,128)(2,1)}, u32[]{:S(2)}) copy-start(bf16[16,256]{1,0:T(8,128)(2,1)} %param.15) | copy-start | bytes 24580
  22.1 9.5 %all-to-all-start.1 = ((bf16[8,16,128]{2,1,0:T(8,128)(2,1)}), bf16[8,16,128]{2,1,0:T(8,128)(2,1)S(1)}, u32[]{:S(2)}, u32[]{:S(2)}) async-start(bf16[8,16,128]{2,1,0:T(8,128)(2,1)} %broadcast_in_dim.13), calls=%async_computation.1 | async-start | bytes 65536 | tf_op jit(solution)/shard_map/all_to_all | solution.py:24
  26.9 21.9 %collective-permute-start = (bf16[2,256,128]{1,2,0:T(8,128)(2,1)S(1)}, bf16[2,256,128]{1,2,0:T(8,128)(2,1)S(1)}, u32[]{:S(2)}, u32[]{:S(2)}) collective-permute-start(bf16[2,256,128]{1,2,0:T(8,128)(2,1)S(1)} %get-tuple-element.36), channel_id=1, source_target_pairs={{0,8},{8,16},{16,24},{24,0},{1,9},{9,17},{17,25},{25,1},{2,10},{10... | collective-permute-start | bytes 393224 | tf_op jit(solution)/shard_map/ppermute | solution.py:31
  32.5 27.5 %all-to-all-start.2 = ((bf16[32,8,256]{2,1,0:T(8,128)(2,1)}), bf16[32,8,256]{2,1,0:T(8,128)(2,1)S(1)}, u32[]{:S(2)}, u32[]{:S(2)}) async-start(bf16[32,8,256]{2,1,0:T(8,128)(2,1)} %bitcast.9), calls=%async_computation.2 | async-start | bytes 262144 | tf_op jit(solution)/shard_map/all_to_all | solution.py:114
  44.1 7.2 %collective-permute-start.1 = (bf16[2,256,128]{1,2,0:T(8,128)(2,1)S(1)}, bf16[2,256,128]{1,2,0:T(8,128)(2,1)S(1)}, u32[]{:S(2)}, u32[]{:S(2)}) collective-permute-start(bf16[2,256,128]{1,2,0:T(8,128)(2,1)S(1)} %get-tuple-element.36), channel_id=1, source_target_pairs={{0,24},{8,0},{16,8},{24,16},{1,25},{9,1},{17,9},{25,17},{2,26},{10... | collective-permute-start | bytes 393224 | tf_op jit(solution)/shard_map/ppermute | solution.py:31
  48.8 7.6 %collective-permute-start.2 = (bf16[2,256,128]{1,2,0:T(8,128)(2,1)S(1)}, bf16[2,256,128]{1,2,0:T(8,128)(2,1)S(1)}, u32[]{:S(2)}, u32[]{:S(2)}) collective-permute-start(bf16[2,256,128]{1,2,0:T(8,128)(2,1)S(1)} %collective-permute-done), channel_id=1, source_target_pairs={{0,8},{8,16},{16,24},{24,0},{1,9},{9,17},{17,25},{25,1},{2,10},{10... | collective-permute-start | bytes 393224 | tf_op jit(solution)/shard_map/ppermute | solution.py:31
  56.6 4.4 %collective-permute-start.3 = (bf16[4,256,128]{1,2,0:T(8,128)(2,1)S(1)}, bf16[4,256,128]{1,2,0:T(8,128)(2,1)S(1)}, u32[]{:S(2)}, u32[]{:S(2)}) collective-permute-start(bf16[4,256,128]{1,2,0:T(8,128)(2,1)S(1)} %get-tuple-element.30), channel_id=1, source_target_pairs={{0,1},{1,0},{2,3},{3,2},{4,5},{5,4},{6,7},{7,6},{8,9},{9,8},{10,11... | collective-permute-start | bytes 786440 | tf_op jit(solution)/shard_map/ppermute | solution.py:31
  62.4 13.4 %all-to-all-start.3 = ((bf16[4,128,640]{2,1,0:T(8,128)(2,1)}), bf16[4,128,640]{2,1,0:T(8,128)(2,1)S(1)}, u32[]{:S(2)}, u32[]{:S(2)}) async-start(bf16[4,128,640]{2,1,0:T(8,128)(2,1)} %broadcast_in_dim.16), calls=%async_computation.3 | async-start | bytes 1310720 | tf_op jit(solution)/shard_map/all_to_all | solution.py:24
  65.9 10.2 %collective-permute-start.4 = (bf16[4,256,128]{1,2,0:T(8,128)(2,1)S(1)}, bf16[4,256,128]{1,2,0:T(8,128)(2,1)S(1)}, u32[]{:S(2)}, u32[]{:S(2)}) collective-permute-start(bf16[4,256,128]{1,2,0:T(8,128)(2,1)S(1)} %get-tuple-element.31), channel_id=1, source_target_pairs={{0,1},{1,0},{2,3},{3,2},{4,5},{5,4},{6,7},{7,6},{8,9},{9,8},{10,11... | collective-permute-start | bytes 786440 | tf_op jit(solution)/shard_map/ppermute | solution.py:31
  75.9 15.0 %copy-start.6 = (f32[16,128]{1,0:T(8,128)S(1)}, f32[16,128]{1,0:T(8,128)}, u32[]{:S(2)}) copy-start(f32[16,128]{1,0:T(8,128)} %copy-done.5) | copy-start | bytes 24580
  75.9 15.0 %copy-start.9 = (f32[16]{0:T(128)S(1)}, f32[16]{0:T(128)}, u32[]{:S(2)}) copy-start(f32[16]{0:T(128)} %copy-done.8) | copy-start | bytes 196
  77.2 29.5 %all-to-all-start.4 = ((bf16[32,8,256]{2,1,0:T(8,128)(2,1)}), bf16[32,8,256]{2,1,0:T(8,128)(2,1)S(1)}, u32[]{:S(2)}, u32[]{:S(2)}) async-start(bf16[32,8,256]{2,1,0:T(8,128)(2,1)} %bitcast.38), calls=%async_computation.4 | async-start | bytes 262144 | tf_op jit(solution)/shard_map/all_to_all | solution.py:147

commit v2 on v1

v2 whole, which is shorter than its diff:
```python
import jax
import jax.numpy as jnp
from jax import lax
from jax.experimental import pallas as pl
from jax.experimental.pallas import tpu as pltpu
from jax.sharding import Mesh
from jax.sharding import PartitionSpec as P

KV = ("z", "y")
TP = ("x", "c")
NEAR = ("z", "c")
epsilon = 1e-06
f32 = jnp.float32
bf16 = jnp.bfloat16
VMEM = pl.BlockSpec(memory_space=pltpu.VMEM)
SMEM = pl.BlockSpec(memory_space=pltpu.SMEM)
HBM = pl.BlockSpec(memory_space=pltpu.HBM)


def shifted(array, axis, step):
    size = lax.axis_size(axis)
    return lax.ppermute(array, axis, [(i, (i + step) % size) for i in range(size)])


def exchanged(array, axes):
    return lax.all_to_all(array, axes, 0, 0, tiled=True)


def matmul(a, b):
    return lax.dot_general(a, b, (((1,), (0,)), ((), ())), preferred_element_type=f32)


def matmul_rows(a, b, precision=None):
    return lax.dot_general(
        a, b, (((1,), (1,)), ((), ())), preferred_element_type=f32, precision=precision
    )


def prepare(
    head_ref,
    bias_ref,
    up_source,
    mlp_gain_source,
    down_source,
    gates_source,
    gain_source,
    norm_source,
    max_source,
    query_source,
    key_source,
    value_source,
    outgate_source,
    state_source,
    query_ref,
    key_ref,
    value_ref,
    outgate_ref,
    state_ref,
    gates_ref,
    small_ref,
    block_ref,
    up_ref,
    mlp_gain_ref,
    down_ref,
    all_gates_ref,
    gain_ref,
    norm_ref,
    max_ref,
    semaphores,
):
    pairs = (
        (up_source, up_ref),
        (mlp_gain_source, mlp_gain_ref),
        (down_source, down_ref),
        (gates_source, all_gates_ref),
        (gain_source, gain_ref),
        (norm_source, norm_ref),
        (max_source, max_ref),
        (query_source, query_ref),
        (key_source, key_ref),
        (value_source, value_ref),
        (outgate_source, outgate_ref),
        (state_source, state_ref),
    )
    copies = [
        pltpu.make_async_copy(source, target, semaphores.at[index])
        for index, (source, target) in enumerate(pairs)
    ]
    for copy in copies:
        copy.start()
    for copy in copies[:7]:
        copy.wait()
    half = mlp_gain_ref.shape[1]
    turned = up_ref[...].astype(f32).T
    gain = mlp_gain_ref[...].astype(f32)
    for index in range(mlp_gain_ref.shape[0]):
        span = slice(index * half, (index + 1) * half)
        block_ref[0, :, span] = (turned[:, span] * gain[index : index + 1]).astype(bf16)
    block_ref[1] = down_ref[...]
    head = head_ref[0]
    for kind in range(2):
        gates_ref[kind : kind + 1] = gate_row(all_gates_ref[kind], head)
    rows = gain_ref.shape[0]
    sequences = norm_ref.shape[0]
    small_ref[:rows] = gain_ref[...].astype(f32)
    small_ref[rows : rows + sequences] = norm_ref[...]
    small_ref[rows + sequences :] = jnp.full(
        (small_ref.shape[0] - rows - sequences, small_ref.shape[1]), bias_ref[head], f32
    )
    small_ref[rows + sequences : rows + sequences + 1, :sequences] = max_ref[...]
    for copy in copies[7:]:
        copy.wait()


def gate_row(gates, head):
    mine = lax.broadcasted_iota(jnp.int32, gates.shape, 0) == head
    return jnp.sum(jnp.where(mine, gates.astype(f32), 0.0), axis=0, keepdims=True)


def cell(
    tiles_ref,
    query_ref,
    key_ref,
    value_ref,
    outgate_ref,
    state_ref,
    gates_ref,
    small_ref,
    mixed_ref,
    next_norm_ref,
    next_max_ref,
    kept_ref,
    added_ref,
    value_out_ref,
):
    tiles, sequences, part = tiles_ref.shape
    width = tiles * part
    dim = query_ref.shape[1]
    accumulated = [jnp.zeros((sequences, dim), f32) for _ in range(4)]
    squares = jnp.zeros((sequences, 1), f32)
    gate_in = jnp.zeros((sequences, 1), f32)
    gate_forget = jnp.zeros((sequences, 1), f32)
    lanes = small_ref.shape[1]
    rows = width // lanes
    gain = small_ref[:rows]
    norm = small_ref[rows : rows + sequences]
    bias = small_ref[rows + sequences + 1 : rows + sequences + 2, :1]
    most = small_ref[rows + sequences : rows + sequences + 1, :sequences]
    for index in range(tiles):
        span = slice(index * part, (index + 1) * part)
        values = tiles_ref[index].astype(f32)
        squares += jnp.sum(values * values, axis=1, keepdims=True)
        row = index * part // lanes
        gains = jnp.concatenate([gain[row + k : row + k + 1] for k in range(part // lanes)], axis=1)
        scaled = (values * gains).astype(bf16)
        wide = scaled.astype(f32)
        gate_in += jnp.sum(wide * gates_ref[0:1, span], axis=1, keepdims=True)
        gate_forget += jnp.sum(wide * gates_ref[1:2, span], axis=1, keepdims=True)
        for slot, weight_ref in enumerate((query_ref, key_ref, value_ref, outgate_ref)):
            accumulated[slot] += matmul(scaled, weight_ref[span, :])
    scale = lax.rsqrt(squares / width + epsilon)
    query = accumulated[0] * scale
    key = accumulated[1] * scale * dim ** (-0.5)
    value = accumulated[2] * scale
    outgate = accumulated[3] * scale
    in_gate = gate_in * scale
    forget_log = jax.nn.log_sigmoid(gate_forget * scale + bias)
    square = (sequences, sequences)
    diagonal = lax.broadcasted_iota(jnp.int32, square, 0) == lax.broadcasted_iota(
        jnp.int32, square, 1
    )
    state_max = jnp.sum(jnp.where(diagonal, most, 0.0), axis=1, keepdims=True)
    carried = forget_log + state_max
    next_max = jnp.maximum(carried, in_gate)
    kept = jnp.exp(carried - next_max)
    admitted = jnp.exp(in_gate - next_max)
    added = admitted * key
    next_norm = kept * norm + added
    next_norm_ref[...] = next_norm
    next_max_ref[...] = jnp.sum(jnp.where(diagonal, next_max, 0.0), axis=0, keepdims=True)
    kept_ref[...] = kept
    added_ref[...] = added
    value_out_ref[...] = value
    denominator = jnp.sum(query * next_norm, axis=1, keepdims=True)
    columns = query.T
    read = jnp.concatenate(
        [
            jnp.sum(columns[:, s : s + 1] * state_ref[s], axis=0, keepdims=True)
            for s in range(sequences)
        ],
        axis=0,
    )
    numerator = kept * read + jnp.sum(query * added, axis=1, keepdims=True) * value
    head_out = numerator / jnp.maximum(jnp.abs(denominator), 1.0)
    mixed = (head_out * jax.nn.sigmoid(outgate)).astype(bf16)
    mixed_ref[...] = jnp.broadcast_to(mixed[None], mixed_ref.shape)


def attend(tiles_ref, weight_ref, tokens_ref, residual_ref, outgoing_ref):
    heads, _, dim = tiles_ref.shape
    total = tokens_ref[...].astype(f32)
    attended = jnp.zeros(total.shape, f32)
    for head in range(heads):
        attended += matmul(tiles_ref[head], weight_ref[head * dim : (head + 1) * dim, :])
    residual = (total + attended).astype(bf16)
    residual_ref[...] = residual
    _, cores, share, columns = outgoing_ref.shape
    outgoing_ref[...] = jnp.broadcast_to(
        residual.reshape(1, cores, share, columns), outgoing_ref.shape
    )


def up(core_ref, rows_ref, own0, own1, own2, own3, other_ref, out_ref):
    core = core_ref[0]
    groups, _, share, columns = rows_ref.shape
    count = groups * share
    mine = rows_ref[:, pl.ds(core, 1)].reshape(count, columns)
    theirs = rows_ref[:, pl.ds(1 - core, 1)].reshape(count, columns)
    hidden = other_ref.shape[1]
    pieces = []
    for index, own in enumerate((own0, own1, own2, own3)):
        pieces.append(
            (matmul_rows(mine, own[0]) + matmul_rows(theirs, other_ref[index])).astype(bf16)
        )
    first = mine.astype(f32)
    second = theirs.astype(f32)
    ones = jnp.ones((16, columns), f32)
    squares = matmul_rows(ones, first * first + second * second, lax.Precision.HIGHEST)
    high = squares.astype(bf16)
    low = (squares - high.astype(f32)).astype(bf16)
    for copy in range(out_ref.shape[0]):
        for index, piece in enumerate(pieces):
            out_ref[copy, :count, index * hidden : (index + 1) * hidden] = piece
        out_ref[copy, count:, :count] = high
        out_ref[copy, count:, count : 2 * count] = low
        out_ref[copy, count:, 2 * count :] = jnp.zeros(
            (16, out_ref.shape[2] - 2 * count), bf16
        )


def down(core_ref, sums_ref, own0, own1, own2, own3, other_ref, out_ref):
    core = core_ref[0]
    groups, cores, share, columns = out_ref.shape
    count = groups * share
    hidden = other_ref.shape[1]
    width = columns * cores * sums_ref.shape[0]
    total = jnp.sum(sums_ref[:, :count, :].astype(f32), axis=0)
    tail = jnp.sum(sums_ref[:, count:, : 2 * count].astype(f32), axis=0)
    squares = (tail[:, :count] + tail[:, count:]).T[:, :1]
    scale = lax.rsqrt(squares / width + epsilon)
    active = jnp.maximum(total * scale, 0.0)
    active = (active * active).astype(bf16)
    mine = jnp.zeros((count, columns), f32)
    theirs = jnp.zeros((count, columns), f32)
    for index, own in enumerate((own0, own1, own2, own3)):
        piece = active[:, index * hidden : (index + 1) * hidden]
        mine += matmul(piece, own[1])
        theirs += matmul(piece, other_ref[index])
    out_ref[:, pl.ds(core, 1)] = mine.astype(bf16).reshape(groups, 1, share, columns)
    out_ref[:, pl.ds(1 - core, 1)] = theirs.astype(bf16).reshape(groups, 1, share, columns)


def call(kernel, shapes, specs, scratch=()):
    return pl.pallas_call(
        kernel,
        out_shape=shapes,
        in_specs=specs,
        out_specs=jax.tree.map(lambda _: VMEM, shapes),
        scratch_shapes=scratch,
        compiler_params=pltpu.CompilerParams(vmem_limit_bytes=8 * 2**20),
        cost_estimate=pl.CostEstimate(flops=1000000, bytes_accessed=1000000, transcendentals=0),
    )


def body(
    tokens,
    attn_gain,
    query_weight,
    key_weight,
    value_weight,
    outgate_weight,
    gate_weight,
    forget_bias,
    state_matrix,
    state_norm,
    state_max,
    out_weight,
    mlp_gain,
    up_weight,
    down_weight,
):
    sequences, columns = tokens.shape
    dim = state_matrix.shape[2]
    head = lax.axis_index(TP).reshape(1)
    core = lax.axis_index("c").reshape(1)
    shape = jax.ShapeDtypeStruct
    parts = lax.axis_size(TP)

    tiles = exchanged(jnp.broadcast_to(tokens[None], (parts, *tokens.shape)), TP)

    sources = (
        up_weight,
        mlp_gain.reshape(-1, dim),
        down_weight,
        gate_weight,
        attn_gain.reshape(-1, dim),
        state_norm[:, 0],
        state_max.reshape(1, -1),
    )
    fetched = (query_weight, key_weight, value_weight, outgate_weight, state_matrix[:, 0])
    *fetched, block = call(
        prepare,
        tuple(shape(array.shape, array.dtype) for array in fetched)
        + (
            shape((2, attn_gain.shape[0]), f32),
            shape((attn_gain.shape[0] // dim + sequences + 8, dim), f32),
            shape((2, *down_weight.shape), bf16),
        ),
        [SMEM, SMEM] + [HBM] * (len(sources) + len(fetched)),
        scratch=[pltpu.VMEM(array.shape, array.dtype) for array in sources]
        + [pltpu.SemaphoreType.DMA((len(sources) + len(fetched),))],
    )(
        head,
        forget_bias,
        *(pltpu.with_memory_space_constraint(array, pltpu.HBM) for array in sources + fetched),
    )
    following = shifted(block, "y", 1)
    preceding = shifted(block, "y", -1)
    opposite = shifted(following, "y", 1)
    own = (block, following, preceding, opposite)
    up_other = shifted(jnp.stack([part[0] for part in own]), "c", 1)
    down_other = shifted(jnp.stack([part[1] for part in own]), "c", 1)

    mixed, next_norm, next_max, kept, added, value = call(
        cell,
        (
            shape((parts, sequences, dim), bf16),
            shape((sequences, dim), f32),
            shape((1, sequences), f32),
            shape((sequences, 1), f32),
            shape((sequences, dim), f32),
            shape((sequences, dim), f32),
        ),
        [VMEM] * 8,
    )(tiles, *fetched)
    next_matrix = (
        kept[:, :, None] * state_matrix[:, 0] + added[:, :, None] * value[:, None, :]
    )
    mixed = exchanged(mixed, TP)

    cores = lax.axis_size("c")
    groups = lax.axis_size("z")
    share = sequences // cores
    residual, outgoing = call(
        attend,
        (shape((sequences, columns), bf16), shape((groups, cores, share, columns), bf16)),
        [VMEM] * 3,
    )(mixed, out_weight, tokens)
    rows = exchanged(outgoing.reshape(groups * cores, share, columns), NEAR)
    count = groups * share
    hidden = down_weight.shape[0] * len(own)
    sums = call(
        up, shape((lax.axis_size("x"), count + 16, hidden), bf16), [SMEM] + [VMEM] * 6
    )(core, rows.reshape(groups, cores, share, columns), *own, up_other)
    sums = exchanged(sums, "x")
    back = call(down, shape((groups, cores, share, columns), bf16), [SMEM] + [VMEM] * 6)(
        core, sums, *own, down_other
    )
    back = exchanged(back.reshape(groups * cores, share, columns), NEAR)
    mixer_out = jnp.sum(back.reshape(groups, cores, share, columns).astype(f32), axis=0)
    result = (residual.astype(f32) + mixer_out.reshape(sequences, columns)).astype(bf16)
    return (result, next_matrix[:, None], next_norm[:, None], next_max.reshape(-1, 1))


def solution(mesh):
    split = Mesh(mesh.devices.reshape(16, 4, 4, 2), ("z", "y", "x", "c"))
    placed = (
        P(KV, TP),
        P(),
        P(None, TP),
        P(None, TP),
        P(None, TP),
        P(None, TP),
        P(),
        P(),
        P(KV, TP, None, None),
        P(KV, TP, None),
        P(KV, TP),
        P(None, TP),
        P(TP),
        P(TP, KV),
        P(KV, TP),
    )
    return jax.shard_map(
        body,
        mesh=split,
        in_specs=placed,
        out_specs=(P(KV, TP), P(KV, TP, None, None), P(KV, TP, None), P(KV, TP)),
        check_vma=False,
    )
```

time: 108 us -> 107 us (level)
  Pallas kernels: 0 us -> 7.34 us
  other arithmetic: 6.74 us -> 2.15 us
  waiting for transfers between devices: 30.7 us -> 34.6 us
  local copies, waits for them, and re-layouts: 7.76 us -> 4.9 us
  matrix products: 2.6 us -> 0 us
  starting transfers between devices: 58.5 us -> 56.5 us
    pallas_call x0 -> x5, Pallas kernels: none -> 7.34 us  [the longest x1 2.68 us: body(): call(prepare, tuple((shape(array.shape, array.dtype) for array in fetched...]
    unnamed x29 -> x12, local copies, waits for them, and re-layouts: 1.03 us -> 3.53 us
    broadcast_in_dim x4 -> x1, local copies, waits for them, and re-layouts: 3.6 us -> 1.33 us  [body(): jnp.broadcast_to(tokens[None], (parts, *tokens.shape))]
    ppermute x5, waiting for transfers between devices: 6.29 us -> 8.51 us  [shifted(): lax.ppermute(array, axis, [(i, (i + step) % size) for i in range(size)])]
    dot_general x8 -> x0, matrix products: 2.15 us -> none  [the longest x4 1.37 us: product(): return jnp.dot(scaled, weight, preferred_element_type=f32)]
    dynamic_slice x2 -> x0, local copies, waits for them, and re-layouts: 2.1 us -> none  [the longest x1 1.24 us: body(): my_bias = lax.dynamic_index_in_dim(forget_bias, head, 0, keepdims=True)]
    all_to_all x5, waiting for transfers between devices: 24.4 us -> 26.1 us  [exchanged(): return lax.all_to_all(array, axes, 0, 0, tiled=True)]
    convert_element_type x5 -> x0, other arithmetic: 1.4 us -> none  [the longest x2 0.7 us: body(): scaled = (values * attn_gain.astype(f32)).astype(bf16)]
  transfers between devices with their start and end apart: 10 -> 10, of which waited for: 7 -> 7; matrix products, arithmetic and copies ran while one was open for 8% -> 1% of each run, Pallas kernels for 0% -> 5%
where the time goes in v2:
time: 107 us; the launch traced here: 106 us
  starting transfers between devices  56.5 us (53%)
  waiting for transfers between devices  34.6 us (32%)
  Pallas kernels  7.34 us (7%)
  local copies, waits for them, and re-layouts  4.9 us (5%)
  other arithmetic  2.15 us (2%)
    all_to_all x5, starting transfers between devices, exchanged(): return lax.all_to_all(array, axes, 0, 0, tiled=True)  42.7 us
    all_to_all x5, waiting for transfers between devices, exchanged(): return lax.all_to_all(array, axes, 0, 0, tiled=True)  26.1 us
    ppermute x5, starting transfers between devices, shifted(): lax.ppermute(array, axis, [(i, (i + step) % size) for i in range(size)])  13.8 us
    ppermute x5, waiting for transfers between devices, shifted(): lax.ppermute(array, axis, [(i, (i + step) % size) for i in range(size)])  8.51 us
    unnamed x12, local copies, waits for them, and re-layouts  3.53 us
    pallas_call x1, Pallas kernels, body(): call(prepare, tuple((shape(array.shape, array.dtype) for array in fetched...  2.68 us
  transfers between devices with their start and end apart: 10, of which 7 were waited for; matrix products, arithmetic and copies ran while one was open for 1% of the time, Pallas kernels for 5%

profile of v2, /device:TPU:1, one launch (start us, length us, event | category | flops | bytes accessed | tf_op | source)
XLA Modules:
  0.0 106.3 jit_solution(16886993995182529678)
XLA Ops:
  0.6 1.3 %broadcast_in_dim.4 = bf16[8,16,256]{2,1,0:T(8,128)(2,1)} broadcast(bf16[16,256]{1,0:T(8,128)(2,1)} %tokens_ref.1), dimensions={1,2} | broadcast | bytes 73728 | tf_op jit(solution)/shard_map/broadcast_in_dim | solution.py:299
  2.0 10.1 %all-to-all-start = ((bf16[8,16,256]{2,1,0:T(8,128)(2,1)}), bf16[8,16,256]{2,1,0:T(8,128)(2,1)S(1)}, u32[]{:S(2)}, u32[]{:S(2)}) async-start(bf16[8,16,256]{2,1,0:T(8,128)(2,1)} %broadcast_in_dim.4), calls=%async_computation | async-start | bytes 131072 | tf_op jit(solution)/shard_map/all_to_all | solution.py:26
  12.0 0.0 copy-start.4
  12.0 0.7 copy-done.4
  12.7 2.7 %shard_map.174 = (bf16[2048,128]{1,0:T(8,128)(2,1)S(1)}, bf16[2048,128]{1,0:T(8,128)(2,1)S(1)}, bf16[2048,128]{1,0:T(8,128)(2,1)S(1)}, bf16[2048,128]{1,0:T(8,12...) custom-call(s32[1]{0:T(128)} %bitcast.head_ref, ...), custom_call_target="tpu_custom_call" | custom-call | flops 1000000 | bytes 1000000 | tf_op jit(solution)/shard_map/pallas_call | solution.py:311
  15.4 0.0 copy-start
  15.4 0.8 copy-done
  16.2 1.9 %collective-permute-start.1 = (bf16[2,128,256]{2,1,0:T(8,128)(2,1)S(1)}, bf16[2,128,256]{2,1,0:T(8,128)(2,1)S(1)}, u32[]{:S(2)}, u32[]{:S(2)}) collective-permute-start(bf16[2,128,256]{2,1,0:T(8,128)(2,1)S(1)} %get-tuple-element.30.own0), channel_id=1, source_target_pairs={{0,24},{8,0},{16,8},{24,16},{1,25},{9,1},{17,9},{25,17},{2,26},{10... | collective-permute-start | bytes 393224 | tf_op jit(solution)/shard_map/ppermute | solution.py:22
  18.1 3.4 %collective-permute-start = (bf16[2,128,256]{2,1,0:T(8,128)(2,1)S(1)}, bf16[2,128,256]{2,1,0:T(8,128)(2,1)S(1)}, u32[]{:S(2)}, u32[]{:S(2)}) collective-permute-start(bf16[2,128,256]{2,1,0:T(8,128)(2,1)S(1)} %get-tuple-element.30.own0), channel_id=1, source_target_pairs={{0,8},{8,16},{16,24},{24,0},{1,9},{9,17},{17,25},{25,1},{2,10},{10... | collective-permute-start | bytes 393224 | tf_op jit(solution)/shard_map/ppermute | solution.py:22
  21.5 0.0 all-to-all-done.tiles_ref
  21.5 0.0 copy-start.1
  21.5 1.0 copy-done.1
  22.5 1.5 %shard_map.175 = (bf16[8,16,128]{2,1,0:T(8,128)(2,1)}, f32[16,128]{1,0:T(8,128)}, f32[1,16]{1,0:T(1,128)}, f32[16,1]{1,0:T(8,128)S(1)}, f32[16,128]{1,0:T(8,128)S(1)}, /*index=5*/f32[16,128]{1,0:T(8,128)S(1)}) custom-call(bf16[8,16,256]{2,1,0:T(8,128)(2,1)S(1)} %all-to-all-done.tiles_ref, bf16[2048,128]{1,0:T(8,128)(2,1)S(1)} %get-tuple-element.20.query_ref, ...), custom_call_target="tpu_custom_call" | custom-call | flops 1000000 | bytes 1000000 | tf_op jit(solution)/shard_map/pallas_call | solution.py:334
  24.1 5.4 %all-to-all-start.1 = ((bf16[8,16,128]{2,1,0:T(8,128)(2,1)}), bf16[8,16,128]{2,1,0:T(8,128)(2,1)S(1)}, u32[]{:S(2)}, u32[]{:S(2)}) async-start(bf16[8,16,128]{2,1,0:T(8,128)(2,1)} %get-tuple-element.27), calls=%async_computation.1 | async-start | bytes 65536 | tf_op jit(solution)/shard_map/all_to_all | solution.py:26
  29.4 0.0 copy-start.3
  29.5 4.7 %all-to-all-done.1.tiles_ref = bf16[8,16,128]{2,1,0:T(8,128)(2,1)S(1)} async-done(((bf16[8,16,128]{2,1,0:T(8,128)(2,1)}), bf16[8,16,128]{2,1,0:T(8,128)(2,1)S(1)}, u32[]{:S(2)}, u32[]{:S(2)}) %all-to-all-start.1) | async-done | bytes 32800 | tf_op jit(solution)/shard_map/all_to_all | solution.py:26
  34.2 0.0 copy-done.3
  34.2 0.0 copy-start.2
  34.2 1.0 copy-done.2
  35.2 0.8 shard_map.176
  36.1 12.7 %all-to-all-start.2 = ((bf16[32,8,256]{2,1,0:T(8,128)(2,1)}), bf16[32,8,256]{2,1,0:T(8,128)(2,1)S(1)}, u32[]{:S(2)}, u32[]{:S(2)}) async-start(bf16[32,8,256]{2,1,0:T(8,128)(2,1)} %bitcast.7), calls=%async_computation.2 | async-start | bytes 262144 | tf_op jit(solution)/shard_map/all_to_all | solution.py:26
  48.7 0.0 collective-permute-done.own1
  48.7 2.2 %collective-permute-start.2 = (bf16[2,128,256]{2,1,0:T(8,128)(2,1)S(1)}, bf16[2,128,256]{2,1,0:T(8,128)(2,1)S(1)}, u32[]{:S(2)}, u32[]{:S(2)}) collective-permute-start(bf16[2,128,256]{2,1,0:T(8,128)(2,1)S(1)} %collective-permute-done.own1), channel_id=1, source_target_pairs={{0,8},{8,16},{16,24},{24,0},{1,9},{9,17},{17,25},{25,1},{2,10},{10... | collective-permute-start | bytes 393224 | tf_op jit(solution)/shard_map/ppermute | solution.py:22
  51.0 0.0 collective-permute-done.1.own2
  51.0 6.2 %collective-permute-done.2.own3 = bf16[2,128,256]{2,1,0:T(8,128)(2,1)S(1)} collective-permute-done((bf16[2,128,256]{2,1,0:T(8,128)(2,1)S(1)}, bf16[2,128,256]{2,1,0:T(8,128)(2,1)S(1)}, u32[]{:S(2)}, u32[]{:S(2)}) %collective-permute-start.2) | collective-permute-done | bytes 131104 | tf_op jit(solution)/shard_map/ppermute | solution.py:22
  57.3 2.7 %collective-permute-start.3 = (bf16[4,128,256]{2,1,0:T(8,128)(2,1)S(1)}, bf16[4,128,256]{2,1,0:T(8,128)(2,1)S(1)}, u32[]{:S(2)}, u32[]{:S(2)}) collective-permute-start(bf16[4,128,256]{2,1,0:T(8,128)(2,1)S(1)} %pad_maximum_fusion), channel_id=1, source_target_pairs={{0,1},{1,0},{2,3},{3,2},{4,5},{5,4},{6,7},{7,6},{8,9},{9,8},{10,11... | collective-permute-start | bytes 786440 | tf_op jit(solution)/shard_map/ppermute | solution.py:22
  60.0 1.1 %collective-permute-done.3.other_ref = bf16[4,128,256]{2,1,0:T(8,128)(2,1)S(1)} collective-permute-done((bf16[4,128,256]{2,1,0:T(8,128)(2,1)S(1)}, bf16[4,128,256]{2,1,0:T(8,128)(2,1)S(1)}, u32[]{:S(2)}, u32[]{:S(2)}) %collective-permute-start.3) | collective-permute-done | bytes 262176 | tf_op jit(solution)/shard_map/ppermute | solution.py:22
  61.1 3.4 %all-to-all-done.2 = bf16[32,8,256]{2,1,0:T(8,128)(2,1)S(1)} async-done(((bf16[32,8,256]{2,1,0:T(8,128)(2,1)}), bf16[32,8,256]{2,1,0:T(8,128)(2,1)S(1)}, u32[]{:S(2)}, u32[]{:S(2)}) %all-to-all-start.2) | async-done | bytes 131104 | tf_op jit(solution)/shard_map/all_to_all | solution.py:26
  64.6 1.2 %shard_map.177 = bf16[4,144,512]{2,1,0:T(8,128)(2,1)} custom-call(s32[1]{0:T(128)} %bitcast.6.core_ref, bf16[16,2,8,256]{3,2,1,0:T(8,128)(2,1)S(1)} %bitcast.20, bf16[2,128,256]{2,1,0:T(8,128)(2,1)S(1)} %get-tuple-element.30.own0, bf16[2,128,256]{2,1,0:T(8,128)(2,1)S(1)} %collective-permute-done.own1, bf16[2,128,256]{2,1,0:T(8,128)(2,1)S(1)} %collective-permute-done.1.own2, ...), custom_call_target="tpu_custom_call" | custom-call | flops 1000000 | bytes 1000000 | tf_op jit(solution)/shard_map/pallas_call | solution.py:362
  65.8 3.5 %all-to-all-start.3 = ((bf16[4,144,512]{2,1,0:T(8,128)(2,1)}), bf16[4,144,512]{2,1,0:T(8,128)(2,1)S(1)}, u32[]{:S(2)}, u32[]{:S(2)}) async-start(bf16[4,144,512]{2,1,0:T(8,128)(2,1)} %shard_map.177), calls=%async_computation.3 | async-start | bytes 1179648 | tf_op jit(solution)/shard_map/all_to_all | solution.py:26
  69.3 0.0 copy-start.5
  69.3 3.6 %collective-permute-start.4 = (bf16[4,128,256]{2,1,0:T(8,128)(2,1)S(1)}, bf16[4,128,256]{2,1,0:T(8,128)(2,1)S(1)}, u32[]{:S(2)}, u32[]{:S(2)}) collective-permute-start(bf16[4,128,256]{2,1,0:T(8,128)(2,1)S(1)} %pad_maximum_fusion.1), channel_id=1, source_target_pairs={{0,1},{1,0},{2,3},{3,2},{4,5},{5,4},{6,7},{7,6},{8,9},{9,8},{10,11... | collective-permute-start | bytes 786440 | tf_op jit(solution)/shard_map/ppermute | solution.py:22
  72.9 1.1 %collective-permute-done.4.other_ref = bf16[4,128,256]{2,1,0:T(8,128)(2,1)S(1)} collective-permute-done((bf16[4,128,256]{2,1,0:T(8,128)(2,1)S(1)}, bf16[4,128,256]{2,1,0:T(8,128)(2,1)S(1)}, u32[]{:S(2)}, u32[]{:S(2)}) %collective-permute-start.4) | collective-permute-done | bytes 262176 | tf_op jit(solution)/shard_map/ppermute | solution.py:22
  74.1 3.6 %all-to-all-done.3.sums_ref = bf16[4,144,512]{2,1,0:T(8,128)(2,1)S(1)} async-done(((bf16[4,144,512]{2,1,0:T(8,128)(2,1)}), bf16[4,144,512]{2,1,0:T(8,128)(2,1)S(1)}, u32[]{:S(2)}, u32[]{:S(2)}) %all-to-all-start.3) | async-done | bytes 589856 | tf_op jit(solution)/shard_map/all_to_all | solution.py:26
  77.6 1.1 %shard_map.178 = bf16[16,2,8,256]{3,2,1,0:T(8,128)(2,1)} custom-call(s32[1]{0:T(128)} %bitcast.6.core_ref, bf16[4,144,512]{2,1,0:T(8,128)(2,1)S(1)} %all-to-all-done.3.sums_ref, bf16[2,128,256]{2,1,0:T(8,128)(2,1)S(1)} %get-tuple-element.30.own0, bf16[2,128,256]{2,1,0:T(8,128)(2,1)S(1)} %collective-permute-done.own1, ...), custom_call_target="tpu_custom_call" | custom-call | flops 1000000 | bytes 1000000 | tf_op jit(solution)/shard_map/pallas_call | solution.py:366
  78.7 11.1 %all-to-all-start.4 = ((bf16[32,8,256]{2,1,0:T(8,128)(2,1)}), bf16[32,8,256]{2,1,0:T(8,128)(2,1)S(1)}, u32[]{:S(2)}, u32[]{:S(2)}) async-start(bf16[32,8,256]{2,1,0:T(8,128)(2,1)} %bitcast.9), calls=%async_computation.4 | async-start | bytes 262144 | tf_op jit(solution)/shard_map/all_to_all | solution.py:26
  89.8 0.1 reduce
  89.9 0.0 copy-done.5
  89.9 1.3 %multiply_add_fusion = f32[16,1,128,128]{3,2,1,0:T(8,128)} fusion(f32[16,1,128,128]{3,2,1,0:T(8,128)S(1)} %copy-done.5, f32[16,128]{1,0:T(8,128)S(1)} %get-tuple-element.33, f32[16,128]{1,0:T(8,128)S(1)} %get-tuple-element.32, f32[16]{0:T(128)S(1)} %reduce), kind=kLoop, calls=%fused_computation | loop fusion | flops 786432 | bytes 2113600 | tf_op jit(solution)/shard_map/add | solution.py:347
  91.3 14.4 %all-to-all-done.4 = bf16[32,8,256]{2,1,0:T(8,128)(2,1)S(1)} async-done(((bf16[32,8,256]{2,1,0:T(8,128)(2,1)}), bf16[32,8,256]{2,1,0:T(8,128)(2,1)S(1)}, u32[]{:S(2)}, u32[]{:S(2)}) %all-to-all-start.4) | async-done | bytes 131104 | tf_op jit(solution)/shard_map/all_to_all | solution.py:26
  105.7 0.6 fusion
  (7 shorter events, 0.1 us)
Async XLA Ops:
  2.0 19.5 %all-to-all-start = ((bf16[8,16,256]{2,1,0:T(8,128)(2,1)}), bf16[8,16,256]{2,1,0:T(8,128)(2,1)S(1)}, u32[]{:S(2)}, u32[]{:S(2)}) async-start(bf16[8,16,256]{2,1,0:T(8,128)(2,1)} %broadcast_in_dim.4), calls=%async_computation | async-start | bytes 131072 | tf_op jit(solution)/shard_map/all_to_all | solution.py:26
  12.0 0.7 copy-start.4
  15.4 0.8 copy-start
  16.2 34.8 %collective-permute-start.1 = (bf16[2,128,256]{2,1,0:T(8,128)(2,1)S(1)}, bf16[2,128,256]{2,1,0:T(8,128)(2,1)S(1)}, u32[]{:S(2)}, u32[]{:S(2)}) collective-permute-start(bf16[2,128,256]{2,1,0:T(8,128)(2,1)S(1)} %get-tuple-element.30.own0), channel_id=1, source_target_pairs={{0,24},{8,0},{16,8},{24,16},{1,25},{9,1},{17,9},{25,17},{2,26},{10... | collective-permute-start | bytes 393224 | tf_op jit(solution)/shard_map/ppermute | solution.py:22
  18.1 30.6 %collective-permute-start = (bf16[2,128,256]{2,1,0:T(8,128)(2,1)S(1)}, bf16[2,128,256]{2,1,0:T(8,128)(2,1)S(1)}, u32[]{:S(2)}, u32[]{:S(2)}) collective-permute-start(bf16[2,128,256]{2,1,0:T(8,128)(2,1)S(1)} %get-tuple-element.30.own0), channel_id=1, source_target_pairs={{0,8},{8,16},{16,24},{24,0},{1,9},{9,17},{17,25},{25,1},{2,10},{10... | collective-permute-start | bytes 393224 | tf_op jit(solution)/shard_map/ppermute | solution.py:22
  21.5 1.0 copy-start.1
  24.1 10.1 %all-to-all-start.1 = ((bf16[8,16,128]{2,1,0:T(8,128)(2,1)}), bf16[8,16,128]{2,1,0:T(8,128)(2,1)S(1)}, u32[]{:S(2)}, u32[]{:S(2)}) async-start(bf16[8,16,128]{2,1,0:T(8,128)(2,1)} %get-tuple-element.27), calls=%async_computation.1 | async-start | bytes 65536 | tf_op jit(solution)/shard_map/all_to_all | solution.py:26
  29.4 4.7 %copy-start.3 = (bf16[16,256]{1,0:T(8,128)(2,1)S(1)}, bf16[16,256]{1,0:T(8,128)(2,1)}, u32[]{:S(2)}) copy-start(bf16[16,256]{1,0:T(8,128)(2,1)} %tokens_ref.1) | copy-start | bytes 24580
  34.2 1.0 copy-start.2
  36.1 28.5 %all-to-all-start.2 = ((bf16[32,8,256]{2,1,0:T(8,128)(2,1)}), bf16[32,8,256]{2,1,0:T(8,128)(2,1)S(1)}, u32[]{:S(2)}, u32[]{:S(2)}) async-start(bf16[32,8,256]{2,1,0:T(8,128)(2,1)} %bitcast.7), calls=%async_computation.2 | async-start | bytes 262144 | tf_op jit(solution)/shard_map/all_to_all | solution.py:26
  48.7 8.5 %collective-permute-start.2 = (bf16[2,128,256]{2,1,0:T(8,128)(2,1)S(1)}, bf16[2,128,256]{2,1,0:T(8,128)(2,1)S(1)}, u32[]{:S(2)}, u32[]{:S(2)}) collective-permute-start(bf16[2,128,256]{2,1,0:T(8,128)(2,1)S(1)} %collective-permute-done.own1), channel_id=1, source_target_pairs={{0,8},{8,16},{16,24},{24,0},{1,9},{9,17},{17,25},{25,1},{2,10},{10... | collective-permute-start | bytes 393224 | tf_op jit(solution)/shard_map/ppermute | solution.py:22
  57.3 3.9 %collective-permute-start.3 = (bf16[4,128,256]{2,1,0:T(8,128)(2,1)S(1)}, bf16[4,128,256]{2,1,0:T(8,128)(2,1)S(1)}, u32[]{:S(2)}, u32[]{:S(2)}) collective-permute-start(bf16[4,128,256]{2,1,0:T(8,128)(2,1)S(1)} %pad_maximum_fusion), channel_id=1, source_target_pairs={{0,1},{1,0},{2,3},{3,2},{4,5},{5,4},{6,7},{7,6},{8,9},{9,8},{10,11... | collective-permute-start | bytes 786440 | tf_op jit(solution)/shard_map/ppermute | solution.py:22
  65.8 11.9 %all-to-all-start.3 = ((bf16[4,144,512]{2,1,0:T(8,128)(2,1)}), bf16[4,144,512]{2,1,0:T(8,128)(2,1)S(1)}, u32[]{:S(2)}, u32[]{:S(2)}) async-start(bf16[4,144,512]{2,1,0:T(8,128)(2,1)} %shard_map.177), calls=%async_computation.3 | async-start | bytes 1179648 | tf_op jit(solution)/shard_map/all_to_all | solution.py:26
  69.3 20.7 %copy-start.5 = (f32[16,1,128,128]{3,2,1,0:T(8,128)S(1)}, f32[16,1,128,128]{3,2,1,0:T(8,128)}, u32[]{:S(2)}) copy-start(f32[16,1,128,128]{3,2,1,0:T(8,128)} %param.23) | copy-start | bytes 3145732
  69.3 4.8 %collective-permute-start.4 = (bf16[4,128,256]{2,1,0:T(8,128)(2,1)S(1)}, bf16[4,128,256]{2,1,0:T(8,128)(2,1)S(1)}, u32[]{:S(2)}, u32[]{:S(2)}) collective-permute-start(bf16[4,128,256]{2,1,0:T(8,128)(2,1)S(1)} %pad_maximum_fusion.1), channel_id=1, source_target_pairs={{0,1},{1,0},{2,3},{3,2},{4,5},{5,4},{6,7},{7,6},{8,9},{9,8},{10,11... | collective-permute-start | bytes 786440 | tf_op jit(solution)/shard_map/ppermute | solution.py:22
  78.7 26.9 %all-to-all-start.4 = ((bf16[32,8,256]{2,1,0:T(8,128)(2,1)}), bf16[32,8,256]{2,1,0:T(8,128)(2,1)S(1)}, u32[]{:S(2)}, u32[]{:S(2)}) async-start(bf16[32,8,256]{2,1,0:T(8,128)(2,1)} %bitcast.9), calls=%async_computation.4 | async-start | bytes 262144 | tf_op jit(solution)/shard_map/all_to_all | solution.py:26

commit v3 on v2

--- a/solution.py
+++ b/solution.py
@@ -6,9 +6,9 @@
 from jax.sharding import Mesh
 from jax.sharding import PartitionSpec as P
 
-KV = ("z", "y")
+KV = ("zh", "zl", "y")
 TP = ("x", "c")
-NEAR = ("z", "c")
+NEAR = ("zl", "y", "c")
 epsilon = 1e-06
 f32 = jnp.float32
 bf16 = jnp.bfloat16
@@ -38,7 +38,6 @@
 
 def prepare(
     head_ref,
-    bias_ref,
     up_source,
     mlp_gain_source,
     down_source,
@@ -46,16 +45,17 @@
     gain_source,
     norm_source,
     max_source,
+    bias_source,
     query_source,
     key_source,
     value_source,
     outgate_source,
-    state_source,
+    out_source,
     query_ref,
     key_ref,
     value_ref,
     outgate_ref,
-    state_ref,
+    out_ref,
     gates_ref,
     small_ref,
     block_ref,
@@ -66,6 +66,7 @@
     gain_ref,
     norm_ref,
     max_ref,
+    bias_ref,
     semaphores,
 ):
     pairs = (
@@ -76,11 +77,12 @@
         (gain_source, gain_ref),
         (norm_source, norm_ref),
         (max_source, max_ref),
+        (bias_source, bias_ref),
         (query_source, query_ref),
         (key_source, key_ref),
         (value_source, value_ref),
         (outgate_source, outgate_ref),
-        (state_source, state_ref),
+        (out_source, out_ref),
     )
     copies = [
         pltpu.make_async_copy(source, target, semaphores.at[index])
@@ -88,7 +90,7 @@
     ]
     for copy in copies:
         copy.start()
-    for copy in copies[:7]:
+    for copy in copies[:8]:
         copy.wait()
     half = mlp_gain_ref.shape[1]
     turned = up_ref[...].astype(f32).T
@@ -104,11 +106,13 @@
     sequences = norm_ref.shape[0]
     small_ref[:rows] = gain_ref[...].astype(f32)
     small_ref[rows : rows + sequences] = norm_ref[...]
-    small_ref[rows + sequences :] = jnp.full(
-        (small_ref.shape[0] - rows - sequences, small_ref.shape[1]), bias_ref[head], f32
+    mine = lax.broadcasted_iota(jnp.int32, bias_ref.shape, 1) == head
+    bias = jnp.sum(jnp.where(mine, bias_ref[...], 0.0), axis=1, keepdims=True)
+    small_ref[rows + sequences :] = jnp.broadcast_to(
+        bias, (small_ref.shape[0] - rows - sequences, small_ref.shape[1])
     )
     small_ref[rows + sequences : rows + sequences + 1, :sequences] = max_ref[...]
-    for copy in copies[7:]:
+    for copy in copies[8:]:
         copy.wait()
 
 
@@ -123,7 +127,7 @@
     key_ref,
     value_ref,
     outgate_ref,
-    state_ref,
+    state_source,
     gates_ref,
     small_ref,
     mixed_ref,
@@ -132,7 +136,11 @@
     kept_ref,
     added_ref,
     value_out_ref,
+    state_ref,
+    semaphore,
 ):
+    fetch = pltpu.make_async_copy(state_source, state_ref, semaphore)
+    fetch.start()
     tiles, sequences, part = tiles_ref.shape
     width = tiles * part
     dim = query_ref.shape[1]
@@ -183,6 +191,7 @@
     value_out_ref[...] = value
     denominator = jnp.sum(query * next_norm, axis=1, keepdims=True)
     columns = query.T
+    fetch.wait()
     read = jnp.concatenate(
         [
             jnp.sum(columns[:, s : s + 1] * state_ref[s], axis=0, keepdims=True)
@@ -218,9 +227,9 @@
     theirs = rows_ref[:, pl.ds(1 - core, 1)].reshape(count, columns)
     hidden = other_ref.shape[1]
     pieces = []
-    for index, own in enumerate((own0, own1, own2, own3)):
+    for index, own in enumerate((own0[0], own1[0], own2[0], own3[...])):
         pieces.append(
-            (matmul_rows(mine, own[0]) + matmul_rows(theirs, other_ref[index])).astype(bf16)
+            (matmul_rows(mine, own) + matmul_rows(theirs, other_ref[index])).astype(bf16)
         )
     first = mine.astype(f32)
     second = theirs.astype(f32)
@@ -252,9 +261,9 @@
     active = (active * active).astype(bf16)
     mine = jnp.zeros((count, columns), f32)
     theirs = jnp.zeros((count, columns), f32)
-    for index, own in enumerate((own0, own1, own2, own3)):
+    for index, own in enumerate((own0[1], own1[1], own2[1], own3[...])):
         piece = active[:, index * hidden : (index + 1) * hidden]
-        mine += matmul(piece, own[1])
+        mine += matmul(piece, own)
         theirs += matmul(piece, other_ref[index])
     out_ref[:, pl.ds(core, 1)] = mine.astype(bf16).reshape(groups, 1, share, columns)
     out_ref[:, pl.ds(1 - core, 1)] = theirs.astype(bf16).reshape(groups, 1, share, columns)
@@ -306,9 +315,10 @@
         attn_gain.reshape(-1, dim),
         state_norm[:, 0],
         state_max.reshape(1, -1),
-    )
-    fetched = (query_weight, key_weight, value_weight, outgate_weight, state_matrix[:, 0])
-    *fetched, block = call(
+        forget_bias.reshape(1, -1),
+    )
+    fetched = (query_weight, key_weight, value_weight, outgate_weight, out_weight)
+    *projections, out_weight, gates, small, block = call(
         prepare,
         tuple(shape(array.shape, array.dtype) for array in fetched)
         + (
@@ -316,20 +326,22 @@
             shape((attn_gain.shape[0] // dim + sequences + 8, dim), f32),
             shape((2, *down_weight.shape), bf16),
         ),
-        [SMEM, SMEM] + [HBM] * (len(sources) + len(fetched)),
+        [SMEM] + [HBM] * (len(sources) + len(fetched)),
         scratch=[pltpu.VMEM(array.shape, array.dtype) for array in sources]
         + [pltpu.SemaphoreType.DMA((len(sources) + len(fetched),))],
     )(
         head,
-        forget_bias,
         *(pltpu.with_memory_space_constraint(array, pltpu.HBM) for array in sources + fetched),
     )
-    following = shifted(block, "y", 1)
-    preceding = shifted(block, "y", -1)
-    opposite = shifted(following, "y", 1)
-    own = (block, following, preceding, opposite)
-    up_other = shifted(jnp.stack([part[0] for part in own]), "c", 1)
-    down_other = shifted(jnp.stack([part[1] for part in own]), "c", 1)
+    following = shifted(block, "zh", 1)
+    preceding = shifted(block, "zh", -1)
+    opposite_up = shifted(following[0], "zh", 1)
+    opposite_down = shifted(preceding[1], "zh", -1)
+    own = (block, following, preceding)
+    up_other = shifted(
+        jnp.stack([block[0], following[0], preceding[0], opposite_up]), "c", 1
+    )
+    down_other = shifted(jnp.stack([block[1], following[1], preceding[1], opposite_down]), "c", 1)
 
     mixed, next_norm, next_max, kept, added, value = call(
         cell,
@@ -341,15 +353,22 @@
             shape((sequences, dim), f32),
             shape((sequences, dim), f32),
         ),
-        [VMEM] * 8,
-    )(tiles, *fetched)
+        [VMEM] * 5 + [HBM] + [VMEM] * 2,
+        scratch=[pltpu.VMEM((sequences, dim, dim), f32), pltpu.SemaphoreType.DMA],
+    )(
+        tiles,
+        *projections,
+        pltpu.with_memory_space_constraint(state_matrix[:, 0], pltpu.HBM),
+        gates,
+        small,
+    )
     next_matrix = (
         kept[:, :, None] * state_matrix[:, 0] + added[:, :, None] * value[:, None, :]
     )
     mixed = exchanged(mixed, TP)
 
     cores = lax.axis_size("c")
-    groups = lax.axis_size("z")
+    groups = lax.axis_size("zl") * lax.axis_size("y")
     share = sequences // cores
     residual, outgoing = call(
         attend,
@@ -358,14 +377,15 @@
     )(mixed, out_weight, tokens)
     rows = exchanged(outgoing.reshape(groups * cores, share, columns), NEAR)
     count = groups * share
-    hidden = down_weight.shape[0] * len(own)
+    hidden = down_weight.shape[0] * up_other.shape[0]
     sums = call(
         up, shape((lax.axis_size("x"), count + 16, hidden), bf16), [SMEM] + [VMEM] * 6
-    )(core, rows.reshape(groups, cores, share, columns), *own, up_other)
+    )(core, rows.reshape(groups, cores, share, columns), *own, opposite_up, up_other)
     sums = exchanged(sums, "x")
     back = call(down, shape((groups, cores, share, columns), bf16), [SMEM] + [VMEM] * 6)(
-        core, sums, *own, down_other
-    )
+        core, sums, *own, opposite_down, down_other
+    )
+    back, next_matrix = lax.optimization_barrier((back, next_matrix))
     back = exchanged(back.reshape(groups * cores, share, columns), NEAR)
     mixer_out = jnp.sum(back.reshape(groups, cores, share, columns).astype(f32), axis=0)
     result = (residual.astype(f32) + mixer_out.reshape(sequences, columns)).astype(bf16)
@@ -373,7 +393,7 @@
 
 
 def solution(mesh):
-    split = Mesh(mesh.devices.reshape(16, 4, 4, 2), ("z", "y", "x", "c"))
+    split = Mesh(mesh.devices.reshape(4, 4, 4, 4, 2), ("zh", "zl", "y", "x", "c"))
     placed = (
         P(KV, TP),
         P(),

time: 107 us -> 101 us (0.944)
  blocking collectives: 0 us -> 20.7 us
  waiting for transfers between devices: 34.6 us -> 14.8 us
  local copies, waits for them, and re-layouts: 4.9 us -> 1.38 us
  starting transfers between devices: 56.5 us -> 54 us
    all_to_all x0 -> x1, blocking collectives: none -> 20.7 us  [exchanged(): return lax.all_to_all(array, axes, 0, 0, tiled=True)]
    all_to_all x5 -> x4, starting transfers between devices: 42.7 us -> 25.2 us  [exchanged(): return lax.all_to_all(array, axes, 0, 0, tiled=True)]
    ppermute x5 -> x6, starting transfers between devices: 13.8 us -> 28.8 us  [shifted(): lax.ppermute(array, axis, [(i, (i + step) % size) for i in range(size)])]
    all_to_all x5 -> x4, waiting for transfers between devices: 26.1 us -> 11.2 us  [exchanged(): return lax.all_to_all(array, axes, 0, 0, tiled=True)]
    ppermute x5 -> x6, waiting for transfers between devices: 8.51 us -> 3.56 us  [shifted(): lax.ppermute(array, axis, [(i, (i + step) % size) for i in range(size)])]
    unnamed x12 -> x4, local copies, waits for them, and re-layouts: 3.53 us -> 0.01 us
  transfers between devices with their start and end apart: 10 -> 10, of which waited for: 7 -> 3; matrix products, arithmetic and copies ran while one was open for 1% -> 2% of each run, Pallas kernels for 5% -> 7%
where the time goes in v3:
time: 101 us
  starting transfers between devices  54 us (53%)
  blocking collectives  20.7 us (20%)
  waiting for transfers between devices  14.8 us (15%)
  Pallas kernels  6.98 us (7%)
  other arithmetic  2.14 us (2%)
  local copies, waits for them, and re-layouts  1.38 us (1%)
    ppermute x6, starting transfers between devices, shifted(): lax.ppermute(array, axis, [(i, (i + step) % size) for i in range(size)])  28.8 us
    all_to_all x4, starting transfers between devices, exchanged(): return lax.all_to_all(array, axes, 0, 0, tiled=True)  25.2 us
    all_to_all x1, blocking collectives, exchanged(): return lax.all_to_all(array, axes, 0, 0, tiled=True)  20.7 us
    all_to_all x4, waiting for transfers between devices, exchanged(): return lax.all_to_all(array, axes, 0, 0, tiled=True)  11.2 us
    ppermute x6, waiting for transfers between devices, shifted(): lax.ppermute(array, axis, [(i, (i + step) % size) for i in range(size)])  3.56 us
    pallas_call x1, Pallas kernels, body(): call(cell, (shape((parts, sequences, dim), bf16), shape((sequences, dim),...  2.53 us
  transfers between devices with their start and end apart: 10, of which 3 were waited for; matrix products, arithmetic and copies ran while one was open for 2% of the time, Pallas kernels for 7%

profile of v3, /device:TPU:1, one launch (start us, length us, event | category | flops | bytes accessed | tf_op | source)
XLA Modules:
  0.0 100.7 jit_solution(15223178159862053237)
XLA Ops:
  0.6 1.3 %broadcast_in_dim.6 = bf16[8,16,256]{2,1,0:T(8,128)(2,1)} broadcast(bf16[16,256]{1,0:T(8,128)(2,1)} %tokens_ref.1), dimensions={1,2} | broadcast | bytes 73728 | tf_op jit(solution)/shard_map/broadcast_in_dim | solution.py:308
  2.0 10.1 %all-to-all-start = ((bf16[8,16,256]{2,1,0:T(8,128)(2,1)}), bf16[8,16,256]{2,1,0:T(8,128)(2,1)S(1)}, u32[]{:S(2)}, u32[]{:S(2)}) async-start(bf16[8,16,256]{2,1,0:T(8,128)(2,1)} %broadcast_in_dim.6), calls=%async_computation | async-start | bytes 131072 | tf_op jit(solution)/shard_map/all_to_all | solution.py:26
  12.1 2.0 %shard_map.174 = (bf16[2048,128]{1,0:T(8,128)(2,1)S(1)}, bf16[2048,128]{1,0:T(8,128)(2,1)S(1)}, bf16[2048,128]{1,0:T(8,128)(2,1)S(1)}, bf16[2048,128]{1,0:T(8,12...) custom-call(s32[1]{0:T(128)} %bitcast.head_ref, ...), custom_call_target="tpu_custom_call" | custom-call | flops 1000000 | bytes 1000000 | tf_op jit(solution)/shard_map/pallas_call | solution.py:321
  14.0 8.2 %collective-permute-start.1 = (bf16[2,128,256]{2,1,0:T(8,128)(2,1)S(1)}, bf16[2,128,256]{2,1,0:T(8,128)(2,1)S(1)}, u32[]{:S(2)}, u32[]{:S(2)}) collective-permute-start(bf16[2,128,256]{2,1,0:T(8,128)(2,1)S(1)} %get-tuple-element.32.own0), channel_id=1, source_target_pairs={{0,384},{128,0},{256,128},{384,256},{1,385},{129,1},{257,129},{385... | collective-permute-start | bytes 393224 | tf_op jit(solution)/shard_map/ppermute | solution.py:22
  22.2 1.9 %collective-permute-start = (bf16[2,128,256]{2,1,0:T(8,128)(2,1)S(1)}, bf16[2,128,256]{2,1,0:T(8,128)(2,1)S(1)}, u32[]{:S(2)}, u32[]{:S(2)}) collective-permute-start(bf16[2,128,256]{2,1,0:T(8,128)(2,1)S(1)} %get-tuple-element.32.own0), channel_id=1, source_target_pairs={{0,128},{128,256},{256,384},{384,0},{1,129},{129,257},{257,385},{3... | collective-permute-start | bytes 393224 | tf_op jit(solution)/shard_map/ppermute | solution.py:22
  24.1 0.0 all-to-all-done.tiles_ref
  24.1 2.5 %shard_map.175 = (bf16[8,16,128]{2,1,0:T(8,128)(2,1)}, f32[16,128]{1,0:T(8,128)}, f32[1,16]{1,0:T(1,128)}, f32[16,1]{1,0:T(8,128)S(1)}, f32[16,128]{1,0:T(8,128)S(1)}, /*index=5*/f32[16,128]{1,0:T(8,128)S(1)}) custom-call(bf16[8,16,256]{2,1,0:T(8,128)(2,1)S(1)} %all-to-all-done.tiles_ref, bf16[2048,128]{1,0:T(8,128)(2,1)S(1)} %get-tuple-element.22.query_ref, ...), custom_call_target="tpu_custom_call" | custom-call | flops 1000000 | bytes 1000000 | tf_op jit(solution)/shard_map/pallas_call | solution.py:346
  26.7 5.1 %all-to-all-start.1 = ((bf16[8,16,128]{2,1,0:T(8,128)(2,1)}), bf16[8,16,128]{2,1,0:T(8,128)(2,1)S(1)}, u32[]{:S(2)}, u32[]{:S(2)}) async-start(bf16[8,16,128]{2,1,0:T(8,128)(2,1)} %get-tuple-element.28), calls=%async_computation.1 | async-start | bytes 65536 | tf_op jit(solution)/shard_map/all_to_all | solution.py:26
  31.8 0.0 copy-start
  31.8 5.0 %all-to-all-done.1.tiles_ref = bf16[8,16,128]{2,1,0:T(8,128)(2,1)S(1)} async-done(((bf16[8,16,128]{2,1,0:T(8,128)(2,1)}), bf16[8,16,128]{2,1,0:T(8,128)(2,1)S(1)}, u32[]{:S(2)}, u32[]{:S(2)}) %all-to-all-start.1) | async-done | bytes 32800 | tf_op jit(solution)/shard_map/all_to_all | solution.py:26
  36.8 0.0 copy-done
  36.8 0.8 shard_map.176
  37.6 6.4 %all-to-all-start.2 = ((bf16[32,8,256]{2,1,0:T(8,128)(2,1)}), bf16[32,8,256]{2,1,0:T(8,128)(2,1)S(1)}, u32[]{:S(2)}, u32[]{:S(2)}) async-start(bf16[32,8,256]{2,1,0:T(8,128)(2,1)} %bitcast.8), calls=%async_computation.2 | async-start | bytes 262144 | tf_op jit(solution)/shard_map/all_to_all | solution.py:26
  44.1 0.0 collective-permute-done.own1
  44.1 6.6 %collective-permute-start.2 = (bf16[128,256]{1,0:T(8,128)(2,1)S(1)}, bf16[128,256]{1,0:T(8,128)(2,1)S(1)}, u32[]{:S(2)}, u32[]{:S(2)}) collective-permute-start(bf16[128,256]{1,0:T(8,128)(2,1)S(1)} %get-tuple-element.51), channel_id=1, source_target_pairs={{0,128},{128,256},{256,384},{384,0},{1,129},{129,257},{257,385},{3... | collective-permute-start | bytes 196616 | tf_op jit(solution)/shard_map/ppermute | solution.py:22
  50.7 0.0 collective-permute-done.1.own2
  50.8 3.5 %collective-permute-done.2.own3 = bf16[128,256]{1,0:T(8,128)(2,1)S(1)} collective-permute-done((bf16[128,256]{1,0:T(8,128)(2,1)S(1)}, bf16[128,256]{1,0:T(8,128)(2,1)S(1)}, u32[]{:S(2)}, u32[]{:S(2)}) %collective-permute-start.2) | collective-permute-done | bytes 65568 | tf_op jit(solution)/shard_map/ppermute | solution.py:22
  54.3 2.7 %collective-permute-start.3 = (bf16[4,128,256]{2,1,0:T(8,128)(2,1)S(1)}, bf16[4,128,256]{2,1,0:T(8,128)(2,1)S(1)}, u32[]{:S(2)}, u32[]{:S(2)}) collective-permute-start(bf16[4,128,256]{2,1,0:T(8,128)(2,1)S(1)} %pad_maximum_fusion), channel_id=1, source_target_pairs={{0,1},{1,0},{2,3},{3,2},{4,5},{5,4},{6,7},{7,6},{8,9},{9,8},{10,11... | collective-permute-start | bytes 786440 | tf_op jit(solution)/shard_map/ppermute | solution.py:22
  57.0 7.2 %collective-permute-start.4 = (bf16[128,256]{1,0:T(8,128)(2,1)S(1)}, bf16[128,256]{1,0:T(8,128)(2,1)S(1)}, u32[]{:S(2)}, u32[]{:S(2)}) collective-permute-start(bf16[128,256]{1,0:T(8,128)(2,1)S(1)} %get-tuple-element.54), channel_id=1, source_target_pairs={{0,384},{128,0},{256,128},{384,256},{1,385},{129,1},{257,129},{385... | collective-permute-start | bytes 196616 | tf_op jit(solution)/shard_map/ppermute | solution.py:22
  64.2 0.0 collective-permute-done.3.other_ref
  64.2 0.0 all-to-all-done.2
  64.2 1.2 %shard_map.177 = bf16[4,144,512]{2,1,0:T(8,128)(2,1)} custom-call(s32[1]{0:T(128)} %bitcast.7.core_ref, bf16[16,2,8,256]{3,2,1,0:T(8,128)(2,1)S(1)} %bitcast.31, bf16[2,128,256]{2,1,0:T(8,128)(2,1)S(1)} %get-tuple-element.32.own0, bf16[2,128,256]{2,1,0:T(8,128)(2,1)S(1)} %collective-permute-done.own1, bf16[2,128,256]{2,1,0:T(8,128)(2,1)S(1)} %collective-permute-done.1.own2, ...), custom_call_target="tpu_custom_call" | custom-call | flops 1000000 | bytes 1000000 | tf_op jit(solution)/shard_map/pallas_call | solution.py:381
  65.4 0.0 copy-start.1
  65.4 3.6 %all-to-all-start.3 = ((bf16[4,144,512]{2,1,0:T(8,128)(2,1)}), bf16[4,144,512]{2,1,0:T(8,128)(2,1)S(1)}, u32[]{:S(2)}, u32[]{:S(2)}) async-start(bf16[4,144,512]{2,1,0:T(8,128)(2,1)} %shard_map.177), calls=%async_computation.3 | async-start | bytes 1179648 | tf_op jit(solution)/shard_map/all_to_all | solution.py:26
  69.1 0.1 reduce
  69.2 0.0 collective-permute-done.4.own3
  69.2 2.2 %collective-permute-start.5 = (bf16[4,128,256]{2,1,0:T(8,128)(2,1)S(1)}, bf16[4,128,256]{2,1,0:T(8,128)(2,1)S(1)}, u32[]{:S(2)}, u32[]{:S(2)}) collective-permute-start(bf16[4,128,256]{2,1,0:T(8,128)(2,1)S(1)} %pad_maximum_fusion.1), channel_id=1, source_target_pairs={{0,1},{1,0},{2,3},{3,2},{4,5},{5,4},{6,7},{7,6},{8,9},{9,8},{10,11... | collective-permute-start | bytes 786440 | tf_op jit(solution)/shard_map/ppermute | solution.py:22
  71.4 0.0 copy-done.1
  71.5 1.3 %multiply_add_fusion = f32[16,128,128]{2,1,0:T(8,128)} fusion(f32[16,128]{1,0:T(8,128)S(1)} %get-tuple-element.35, f32[16,128]{1,0:T(8,128)S(1)} %get-tuple-element.34, f32[16]{0:T(128)S(1)} %reduce, f32[16,1,128,128]{3,2,1,0:T(8,128)S(1)} %copy-done.1), kind=kLoop, calls=%fused_computation | loop fusion | flops 786432 | bytes 2113600 | tf_op jit(solution)/shard_map/add | solution.py:366
  72.8 0.0 collective-permute-done.5.other_ref
  72.8 6.2 %all-to-all-done.3.sums_ref = bf16[4,144,512]{2,1,0:T(8,128)(2,1)S(1)} async-done(((bf16[4,144,512]{2,1,0:T(8,128)(2,1)}), bf16[4,144,512]{2,1,0:T(8,128)(2,1)S(1)}, u32[]{:S(2)}, u32[]{:S(2)}) %all-to-all-start.3) | async-done | bytes 589856 | tf_op jit(solution)/shard_map/all_to_all | solution.py:26
  79.0 0.4 shard_map.178
  79.4 20.7 %all_to_all.25 = bf16[32,8,256]{2,1,0:T(8,128)(2,1)S(1)} all-to-all(bf16[32,8,256]{2,1,0:T(8,128)(2,1)S(1)} %bitcast.32), channel_id=1, replica_groups=mesh['zh'=4,'zl'=4,'y'=4,'x'=4,'c'=2] {'zl','y','c'}, dimensions={0} | all-to-all | bytes 262144 | tf_op jit(solution)/shard_map/all_to_all | solution.py:26
  100.1 0.6 fusion
  (6 shorter events, 0.1 us)
Async XLA Ops:
  2.0 22.2 %all-to-all-start = ((bf16[8,16,256]{2,1,0:T(8,128)(2,1)}), bf16[8,16,256]{2,1,0:T(8,128)(2,1)S(1)}, u32[]{:S(2)}, u32[]{:S(2)}) async-start(bf16[8,16,256]{2,1,0:T(8,128)(2,1)} %broadcast_in_dim.6), calls=%async_computation | async-start | bytes 131072 | tf_op jit(solution)/shard_map/all_to_all | solution.py:26
  14.0 36.7 %collective-permute-start.1 = (bf16[2,128,256]{2,1,0:T(8,128)(2,1)S(1)}, bf16[2,128,256]{2,1,0:T(8,128)(2,1)S(1)}, u32[]{:S(2)}, u32[]{:S(2)}) collective-permute-start(bf16[2,128,256]{2,1,0:T(8,128)(2,1)S(1)} %get-tuple-element.32.own0), channel_id=1, source_target_pairs={{0,384},{128,0},{256,128},{384,256},{1,385},{129,1},{257,129},{385... | collective-permute-start | bytes 393224 | tf_op jit(solution)/shard_map/ppermute | solution.py:22
  22.2 21.9 %collective-permute-start = (bf16[2,128,256]{2,1,0:T(8,128)(2,1)S(1)}, bf16[2,128,256]{2,1,0:T(8,128)(2,1)S(1)}, u32[]{:S(2)}, u32[]{:S(2)}) collective-permute-start(bf16[2,128,256]{2,1,0:T(8,128)(2,1)S(1)} %get-tuple-element.32.own0), channel_id=1, source_target_pairs={{0,128},{128,256},{256,384},{384,0},{1,129},{129,257},{257,385},{3... | collective-permute-start | bytes 393224 | tf_op jit(solution)/shard_map/ppermute | solution.py:22
  26.7 10.1 %all-to-all-start.1 = ((bf16[8,16,128]{2,1,0:T(8,128)(2,1)}), bf16[8,16,128]{2,1,0:T(8,128)(2,1)S(1)}, u32[]{:S(2)}, u32[]{:S(2)}) async-start(bf16[8,16,128]{2,1,0:T(8,128)(2,1)} %get-tuple-element.28), calls=%async_computation.1 | async-start | bytes 65536 | tf_op jit(solution)/shard_map/all_to_all | solution.py:26
  31.8 5.0 %copy-start = (bf16[16,256]{1,0:T(8,128)(2,1)S(1)}, bf16[16,256]{1,0:T(8,128)(2,1)}, u32[]{:S(2)}) copy-start(bf16[16,256]{1,0:T(8,128)(2,1)} %tokens_ref.1) | copy-start | bytes 24580
  37.6 26.6 %all-to-all-start.2 = ((bf16[32,8,256]{2,1,0:T(8,128)(2,1)}), bf16[32,8,256]{2,1,0:T(8,128)(2,1)S(1)}, u32[]{:S(2)}, u32[]{:S(2)}) async-start(bf16[32,8,256]{2,1,0:T(8,128)(2,1)} %bitcast.8), calls=%async_computation.2 | async-start | bytes 262144 | tf_op jit(solution)/shard_map/all_to_all | solution.py:26
  44.1 10.2 %collective-permute-start.2 = (bf16[128,256]{1,0:T(8,128)(2,1)S(1)}, bf16[128,256]{1,0:T(8,128)(2,1)S(1)}, u32[]{:S(2)}, u32[]{:S(2)}) collective-permute-start(bf16[128,256]{1,0:T(8,128)(2,1)S(1)} %get-tuple-element.51), channel_id=1, source_target_pairs={{0,128},{128,256},{256,384},{384,0},{1,129},{129,257},{257,385},{3... | collective-permute-start | bytes 196616 | tf_op jit(solution)/shard_map/ppermute | solution.py:22
  54.3 9.9 %collective-permute-start.3 = (bf16[4,128,256]{2,1,0:T(8,128)(2,1)S(1)}, bf16[4,128,256]{2,1,0:T(8,128)(2,1)S(1)}, u32[]{:S(2)}, u32[]{:S(2)}) collective-permute-start(bf16[4,128,256]{2,1,0:T(8,128)(2,1)S(1)} %pad_maximum_fusion), channel_id=1, source_target_pairs={{0,1},{1,0},{2,3},{3,2},{4,5},{5,4},{6,7},{7,6},{8,9},{9,8},{10,11... | collective-permute-start | bytes 786440 | tf_op jit(solution)/shard_map/ppermute | solution.py:22
  57.0 12.2 %collective-permute-start.4 = (bf16[128,256]{1,0:T(8,128)(2,1)S(1)}, bf16[128,256]{1,0:T(8,128)(2,1)S(1)}, u32[]{:S(2)}, u32[]{:S(2)}) collective-permute-start(bf16[128,256]{1,0:T(8,128)(2,1)S(1)} %get-tuple-element.54), channel_id=1, source_target_pairs={{0,384},{128,0},{256,128},{384,256},{1,385},{129,1},{257,129},{385... | collective-permute-start | bytes 196616 | tf_op jit(solution)/shard_map/ppermute | solution.py:22
  65.4 6.0 %copy-start.1 = (f32[16,1,128,128]{3,2,1,0:T(8,128)S(1)}, f32[16,1,128,128]{3,2,1,0:T(8,128)}, u32[]{:S(2)}) copy-start(f32[16,1,128,128]{3,2,1,0:T(8,128)} %param.23) | copy-start | bytes 3145732
  65.4 13.6 %all-to-all-start.3 = ((bf16[4,144,512]{2,1,0:T(8,128)(2,1)}), bf16[4,144,512]{2,1,0:T(8,128)(2,1)S(1)}, u32[]{:S(2)}, u32[]{:S(2)}) async-start(bf16[4,144,512]{2,1,0:T(8,128)(2,1)} %shard_map.177), calls=%async_computation.3 | async-start | bytes 1179648 | tf_op jit(solution)/shard_map/all_to_all | solution.py:26
  69.2 3.6 %collective-permute-start.5 = (bf16[4,128,256]{2,1,0:T(8,128)(2,1)S(1)}, bf16[4,128,256]{2,1,0:T(8,128)(2,1)S(1)}, u32[]{:S(2)}, u32[]{:S(2)}) collective-permute-start(bf16[4,128,256]{2,1,0:T(8,128)(2,1)S(1)} %pad_maximum_fusion.1), channel_id=1, source_target_pairs={{0,1},{1,0},{2,3},{3,2},{4,5},{5,4},{6,7},{7,6},{8,9},{9,8},{10,11... | collective-permute-start | bytes 786440 | tf_op jit(solution)/shard_map/ppermute | solution.py:22

commit v4 on v3

--- a/solution.py
+++ b/solution.py
@@ -9,6 +9,7 @@
 KV = ("zh", "zl", "y")
 TP = ("x", "c")
 NEAR = ("zl", "y", "c")
+CROSSED = (0, 2, 1, 3)
 epsilon = 1e-06
 f32 = jnp.float32
 bf16 = jnp.bfloat16
@@ -20,6 +21,15 @@
 def shifted(array, axis, step):
     size = lax.axis_size(axis)
     return lax.ppermute(array, axis, [(i, (i + step) % size) for i in range(size)])
+
+
+def crossed(array, step):
+    size = lax.axis_size("zh")
+    pairs = []
+    for plane in range(size):
+        pairs.append((2 * plane, 2 * ((plane + step) % size)))
+        pairs.append((2 * plane + 1, 2 * ((plane - step) % size) + 1))
+    return lax.ppermute(array, ("zh", "c"), pairs)
 
 
 def exchanged(array, axes):
@@ -137,10 +147,19 @@
     added_ref,
     value_out_ref,
     state_ref,
-    semaphore,
+    semaphores,
 ):
-    fetch = pltpu.make_async_copy(state_source, state_ref, semaphore)
-    fetch.start()
+    step = state_ref.shape[0] // semaphores.shape[0]
+    fetches = [
+        pltpu.make_async_copy(
+            state_source.at[pl.ds(index * step, step)],
+            state_ref.at[pl.ds(index * step, step)],
+            semaphores.at[index],
+        )
+        for index in range(semaphores.shape[0])
+    ]
+    for fetch in fetches:
+        fetch.start()
     tiles, sequences, part = tiles_ref.shape
     width = tiles * part
     dim = query_ref.shape[1]
@@ -191,7 +210,8 @@
     value_out_ref[...] = value
     denominator = jnp.sum(query * next_norm, axis=1, keepdims=True)
     columns = query.T
-    fetch.wait()
+    for fetch in fetches:
+        fetch.wait()
     read = jnp.concatenate(
         [
             jnp.sum(columns[:, s : s + 1] * state_ref[s], axis=0, keepdims=True)
@@ -227,9 +247,9 @@
     theirs = rows_ref[:, pl.ds(1 - core, 1)].reshape(count, columns)
     hidden = other_ref.shape[1]
     pieces = []
-    for index, own in enumerate((own0[0], own1[0], own2[0], own3[...])):
+    for index, own in enumerate((own0[0], own1[0], own2[0], own3[0])):
         pieces.append(
-            (matmul_rows(mine, own) + matmul_rows(theirs, other_ref[index])).astype(bf16)
+            (matmul_rows(mine, own) + matmul_rows(theirs, other_ref[CROSSED[index]])).astype(bf16)
         )
     first = mine.astype(f32)
     second = theirs.astype(f32)
@@ -261,10 +281,10 @@
     active = (active * active).astype(bf16)
     mine = jnp.zeros((count, columns), f32)
     theirs = jnp.zeros((count, columns), f32)
-    for index, own in enumerate((own0[1], own1[1], own2[1], own3[...])):
+    for index, own in enumerate((own0[1], own1[1], own2[1], own3[1])):
         piece = active[:, index * hidden : (index + 1) * hidden]
         mine += matmul(piece, own)
-        theirs += matmul(piece, other_ref[index])
+        theirs += matmul(piece, other_ref[CROSSED[index]])
     out_ref[:, pl.ds(core, 1)] = mine.astype(bf16).reshape(groups, 1, share, columns)
     out_ref[:, pl.ds(1 - core, 1)] = theirs.astype(bf16).reshape(groups, 1, share, columns)
 
@@ -333,15 +353,12 @@
         head,
         *(pltpu.with_memory_space_constraint(array, pltpu.HBM) for array in sources + fetched),
     )
-    following = shifted(block, "zh", 1)
-    preceding = shifted(block, "zh", -1)
-    opposite_up = shifted(following[0], "zh", 1)
-    opposite_down = shifted(preceding[1], "zh", -1)
-    own = (block, following, preceding)
-    up_other = shifted(
-        jnp.stack([block[0], following[0], preceding[0], opposite_up]), "c", 1
-    )
-    down_other = shifted(jnp.stack([block[1], following[1], preceding[1], opposite_down]), "c", 1)
+    following = crossed(block, 1)
+    preceding = crossed(block, -1)
+    opposite = crossed(following, 1)
+    own = (block, following, preceding, opposite)
+    up_other = shifted(jnp.stack([part[0] for part in own]), "c", 1)
+    down_other = shifted(jnp.stack([part[1] for part in own]), "c", 1)
 
     mixed, next_norm, next_max, kept, added, value = call(
         cell,
@@ -354,7 +371,7 @@
             shape((sequences, dim), f32),
         ),
         [VMEM] * 5 + [HBM] + [VMEM] * 2,
-        scratch=[pltpu.VMEM((sequences, dim, dim), f32), pltpu.SemaphoreType.DMA],
+        scratch=[pltpu.VMEM((sequences, dim, dim), f32), pltpu.SemaphoreType.DMA((4,))],
     )(
         tiles,
         *projections,
@@ -380,10 +397,10 @@
     hidden = down_weight.shape[0] * up_other.shape[0]
     sums = call(
         up, shape((lax.axis_size("x"), count + 16, hidden), bf16), [SMEM] + [VMEM] * 6
-    )(core, rows.reshape(groups, cores, share, columns), *own, opposite_up, up_other)
+    )(core, rows.reshape(groups, cores, share, columns), *own, up_other)
     sums = exchanged(sums, "x")
     back = call(down, shape((groups, cores, share, columns), bf16), [SMEM] + [VMEM] * 6)(
-        core, sums, *own, opposite_down, down_other
+        core, sums, *own, down_other
     )
     back, next_matrix = lax.optimization_barrier((back, next_matrix))
     back = exchanged(back.reshape(groups * cores, share, columns), NEAR)

time: 101 us -> 95.8 us (0.949)
  starting transfers between devices: 54 us -> 46.8 us
  waiting for transfers between devices: 14.8 us -> 19.1 us
  blocking collectives: 20.7 us -> 17.9 us
    ppermute x6 -> x2, starting transfers between devices: 28.8 us -> 3.96 us  [shifted(): lax.ppermute(array, axis, [(i, (i + step) % size) for i in range(size)])]
    ppermute x0 -> x3, starting transfers between devices: none -> 17.6 us  [crossed(): return lax.ppermute(array, ('zh', 'c'), pairs)]
    ppermute x0 -> x3, waiting for transfers between devices: none -> 6.06 us  [crossed(): return lax.ppermute(array, ('zh', 'c'), pairs)]
    all_to_all x1, blocking collectives: 20.7 us -> 17.9 us  [exchanged(): return lax.all_to_all(array, axes, 0, 0, tiled=True)]
    ppermute x6 -> x2, waiting for transfers between devices: 3.56 us -> 1.54 us  [shifted(): lax.ppermute(array, axis, [(i, (i + step) % size) for i in range(size)])]
  transfers between devices with their start and end apart: 10 -> 9, of which waited for: 3 -> 4; matrix products, arithmetic and copies ran while one was open for 2% -> 2% of each run, Pallas kernels for 7% -> 6%
where the time goes in v4:
time: 95.8 us; the launch traced here: 95.1 us
  starting transfers between devices  46.8 us (49%)
  waiting for transfers between devices  19.1 us (20%)
  blocking collectives  17.9 us (19%)
  Pallas kernels  6.97 us (7%)
  other arithmetic  2.14 us (2%)
  local copies, waits for them, and re-layouts  1.38 us (1%)
    all_to_all x4, starting transfers between devices, exchanged(): return lax.all_to_all(array, axes, 0, 0, tiled=True)  25.2 us
    all_to_all x1, blocking collectives, exchanged(): return lax.all_to_all(array, axes, 0, 0, tiled=True)  17.9 us
    ppermute x3, starting transfers between devices, crossed(): return lax.ppermute(array, ('zh', 'c'), pairs)  17.6 us
    all_to_all x4, waiting for transfers between devices, exchanged(): return lax.all_to_all(array, axes, 0, 0, tiled=True)  11.5 us
    ppermute x3, waiting for transfers between devices, crossed(): return lax.ppermute(array, ('zh', 'c'), pairs)  6.06 us
    ppermute x2, starting transfers between devices, shifted(): lax.ppermute(array, axis, [(i, (i + step) % size) for i in range(size)])  3.96 us
    pallas_call x1, Pallas kernels, body(): call(cell, (shape((parts, sequences, dim), bf16), shape((sequences, dim),...  2.52 us
    pallas_call x1, Pallas kernels, body(): call(prepare, tuple((shape(array.shape, array.dtype) for array in fetched...  1.98 us
  transfers between devices with their start and end apart: 9, of which 4 were waited for; matrix products, arithmetic and copies ran while one was open for 2% of the time, Pallas kernels for 6%

profile of v4, /device:TPU:1, one launch (start us, length us, event | category | flops | bytes accessed | tf_op | source)
XLA Modules:
  0.0 95.1 jit_solution(14490145940903576986)
XLA Ops:
  0.6 1.3 %broadcast_in_dim.6 = bf16[8,16,256]{2,1,0:T(8,128)(2,1)} broadcast(bf16[16,256]{1,0:T(8,128)(2,1)} %tokens_ref.1), dimensions={1,2} | broadcast | bytes 73728 | tf_op jit(solution)/shard_map/broadcast_in_dim | solution.py:328
  2.0 10.1 %all-to-all-start = ((bf16[8,16,256]{2,1,0:T(8,128)(2,1)}), bf16[8,16,256]{2,1,0:T(8,128)(2,1)S(1)}, u32[]{:S(2)}, u32[]{:S(2)}) async-start(bf16[8,16,256]{2,1,0:T(8,128)(2,1)} %broadcast_in_dim.6), calls=%async_computation | async-start | bytes 131072 | tf_op jit(solution)/shard_map/all_to_all | solution.py:36
  12.1 2.0 %shard_map.174 = (bf16[2048,128]{1,0:T(8,128)(2,1)S(1)}, bf16[2048,128]{1,0:T(8,128)(2,1)S(1)}, bf16[2048,128]{1,0:T(8,128)(2,1)S(1)}, bf16[2048,128]{1,0:T(8,12...) custom-call(s32[1]{0:T(128)} %bitcast.head_ref, ...), custom_call_target="tpu_custom_call" | custom-call | flops 1000000 | bytes 1000000 | tf_op jit(solution)/shard_map/pallas_call | solution.py:341
  14.0 4.5 %collective-permute-start.1 = (bf16[2,128,256]{2,1,0:T(8,128)(2,1)S(1)}, bf16[2,128,256]{2,1,0:T(8,128)(2,1)S(1)}, u32[]{:S(2)}, u32[]{:S(2)}) collective-permute-start(bf16[2,128,256]{2,1,0:T(8,128)(2,1)S(1)} %get-tuple-element.32.own0), channel_id=1, source_target_pairs={{0,384},{1,129},{128,0},{129,257},{256,128},{257,385},{384,256},{3... | collective-permute-start | bytes 393224 | tf_op jit(solution)/shard_map/ppermute | solution.py:32
  18.6 5.6 %collective-permute-start = (bf16[2,128,256]{2,1,0:T(8,128)(2,1)S(1)}, bf16[2,128,256]{2,1,0:T(8,128)(2,1)S(1)}, u32[]{:S(2)}, u32[]{:S(2)}) collective-permute-start(bf16[2,128,256]{2,1,0:T(8,128)(2,1)S(1)} %get-tuple-element.32.own0), channel_id=1, source_target_pairs={{0,128},{1,385},{128,256},{129,1},{256,384},{257,129},{384,0},{385... | collective-permute-start | bytes 393224 | tf_op jit(solution)/shard_map/ppermute | solution.py:32
  24.1 0.0 all-to-all-done.tiles_ref
  24.1 2.5 %shard_map.175 = (bf16[8,16,128]{2,1,0:T(8,128)(2,1)}, f32[16,128]{1,0:T(8,128)}, f32[1,16]{1,0:T(1,128)}, f32[16,1]{1,0:T(8,128)S(1)}, f32[16,128]{1,0:T(8,128)S(1)}, /*index=5*/f32[16,128]{1,0:T(8,128)S(1)}) custom-call(bf16[8,16,256]{2,1,0:T(8,128)(2,1)S(1)} %all-to-all-done.tiles_ref, bf16[2048,128]{1,0:T(8,128)(2,1)S(1)} %get-tuple-element.22.query_ref, ...), custom_call_target="tpu_custom_call" | custom-call | flops 1000000 | bytes 1000000 | tf_op jit(solution)/shard_map/pallas_call | solution.py:363
  26.7 5.1 %all-to-all-start.1 = ((bf16[8,16,128]{2,1,0:T(8,128)(2,1)}), bf16[8,16,128]{2,1,0:T(8,128)(2,1)S(1)}, u32[]{:S(2)}, u32[]{:S(2)}) async-start(bf16[8,16,128]{2,1,0:T(8,128)(2,1)} %get-tuple-element.28), calls=%async_computation.1 | async-start | bytes 65536 | tf_op jit(solution)/shard_map/all_to_all | solution.py:36
  31.8 0.0 copy-start
  31.8 5.0 %all-to-all-done.1.tiles_ref = bf16[8,16,128]{2,1,0:T(8,128)(2,1)S(1)} async-done(((bf16[8,16,128]{2,1,0:T(8,128)(2,1)}), bf16[8,16,128]{2,1,0:T(8,128)(2,1)S(1)}, u32[]{:S(2)}, u32[]{:S(2)}) %all-to-all-start.1) | async-done | bytes 32800 | tf_op jit(solution)/shard_map/all_to_all | solution.py:36
  36.8 0.0 copy-done
  36.8 0.8 shard_map.176
  37.6 6.4 %all-to-all-start.2 = ((bf16[32,8,256]{2,1,0:T(8,128)(2,1)}), bf16[32,8,256]{2,1,0:T(8,128)(2,1)S(1)}, u32[]{:S(2)}, u32[]{:S(2)}) async-start(bf16[32,8,256]{2,1,0:T(8,128)(2,1)} %bitcast.8), calls=%async_computation.2 | async-start | bytes 262144 | tf_op jit(solution)/shard_map/all_to_all | solution.py:36
  44.1 0.0 collective-permute-done.own1
  44.1 7.5 %collective-permute-start.2 = (bf16[2,128,256]{2,1,0:T(8,128)(2,1)S(1)}, bf16[2,128,256]{2,1,0:T(8,128)(2,1)S(1)}, u32[]{:S(2)}, u32[]{:S(2)}) collective-permute-start(bf16[2,128,256]{2,1,0:T(8,128)(2,1)S(1)} %collective-permute-done.own1), channel_id=1, source_target_pairs={{0,128},{1,385},{128,256},{129,1},{256,384},{257,129},{384,0},{385... | collective-permute-start | bytes 393224 | tf_op jit(solution)/shard_map/ppermute | solution.py:32
  51.6 0.0 collective-permute-done.1.own2
  51.7 6.1 %collective-permute-done.2.own3 = bf16[2,128,256]{2,1,0:T(8,128)(2,1)S(1)} collective-permute-done((bf16[2,128,256]{2,1,0:T(8,128)(2,1)S(1)}, bf16[2,128,256]{2,1,0:T(8,128)(2,1)S(1)}, u32[]{:S(2)}, u32[]{:S(2)}) %collective-permute-start.2) | collective-permute-done | bytes 131104 | tf_op jit(solution)/shard_map/ppermute | solution.py:32
  57.8 1.9 %collective-permute-start.3 = (bf16[4,128,256]{2,1,0:T(8,128)(2,1)S(1)}, bf16[4,128,256]{2,1,0:T(8,128)(2,1)S(1)}, u32[]{:S(2)}, u32[]{:S(2)}) collective-permute-start(bf16[4,128,256]{2,1,0:T(8,128)(2,1)S(1)} %pad_maximum_fusion), channel_id=1, source_target_pairs={{0,1},{1,0},{2,3},{3,2},{4,5},{5,4},{6,7},{7,6},{8,9},{9,8},{10,11... | collective-permute-start | bytes 786440 | tf_op jit(solution)/shard_map/ppermute | solution.py:23
  59.7 1.5 %collective-permute-done.3.other_ref = bf16[4,128,256]{2,1,0:T(8,128)(2,1)S(1)} collective-permute-done((bf16[4,128,256]{2,1,0:T(8,128)(2,1)S(1)}, bf16[4,128,256]{2,1,0:T(8,128)(2,1)S(1)}, u32[]{:S(2)}, u32[]{:S(2)}) %collective-permute-start.3) | collective-permute-done | bytes 262176 | tf_op jit(solution)/shard_map/ppermute | solution.py:23
  61.2 0.0 all-to-all-done.2
  61.2 1.2 %shard_map.177 = bf16[4,144,512]{2,1,0:T(8,128)(2,1)} custom-call(s32[1]{0:T(128)} %bitcast.7.core_ref, bf16[16,2,8,256]{3,2,1,0:T(8,128)(2,1)S(1)} %bitcast.25, bf16[2,128,256]{2,1,0:T(8,128)(2,1)S(1)} %get-tuple-element.32.own0, bf16[2,128,256]{2,1,0:T(8,128)(2,1)S(1)} %collective-permute-done.own1, bf16[2,128,256]{2,1,0:T(8,128)(2,1)S(1)} %collective-permute-done.1.own2, ...), custom_call_target="tpu_custom_call" | custom-call | flops 1000000 | bytes 1000000 | tf_op jit(solution)/shard_map/pallas_call | solution.py:398
  62.4 0.0 copy-start.1
  62.4 3.6 %all-to-all-start.3 = ((bf16[4,144,512]{2,1,0:T(8,128)(2,1)}), bf16[4,144,512]{2,1,0:T(8,128)(2,1)S(1)}, u32[]{:S(2)}, u32[]{:S(2)}) async-start(bf16[4,144,512]{2,1,0:T(8,128)(2,1)} %shard_map.177), calls=%async_computation.3 | async-start | bytes 1179648 | tf_op jit(solution)/shard_map/all_to_all | solution.py:36
  66.0 0.1 reduce
  66.2 2.0 %collective-permute-start.4 = (bf16[4,128,256]{2,1,0:T(8,128)(2,1)S(1)}, bf16[4,128,256]{2,1,0:T(8,128)(2,1)S(1)}, u32[]{:S(2)}, u32[]{:S(2)}) collective-permute-start(bf16[4,128,256]{2,1,0:T(8,128)(2,1)S(1)} %pad_maximum_fusion.1), channel_id=1, source_target_pairs={{0,1},{1,0},{2,3},{3,2},{4,5},{5,4},{6,7},{7,6},{8,9},{9,8},{10,11... | collective-permute-start | bytes 786440 | tf_op jit(solution)/shard_map/ppermute | solution.py:23
  68.3 0.0 copy-done.1
  68.3 1.3 %multiply_add_fusion = f32[16,128,128]{2,1,0:T(8,128)} fusion(f32[16,128]{1,0:T(8,128)S(1)} %get-tuple-element.35, f32[16,128]{1,0:T(8,128)S(1)} %get-tuple-element.34, f32[16]{0:T(128)S(1)} %reduce, f32[16,1,128,128]{3,2,1,0:T(8,128)S(1)} %copy-done.1), kind=kLoop, calls=%fused_computation | loop fusion | flops 786432 | bytes 2113600 | tf_op jit(solution)/shard_map/add | solution.py:383
  69.6 0.0 collective-permute-done.4.other_ref
  69.6 6.5 %all-to-all-done.3.sums_ref = bf16[4,144,512]{2,1,0:T(8,128)(2,1)S(1)} async-done(((bf16[4,144,512]{2,1,0:T(8,128)(2,1)}), bf16[4,144,512]{2,1,0:T(8,128)(2,1)S(1)}, u32[]{:S(2)}, u32[]{:S(2)}) %all-to-all-start.3) | async-done | bytes 589856 | tf_op jit(solution)/shard_map/all_to_all | solution.py:36
  76.1 0.4 shard_map.178
  76.6 17.9 %all_to_all.25 = bf16[32,8,256]{2,1,0:T(8,128)(2,1)S(1)} all-to-all(bf16[32,8,256]{2,1,0:T(8,128)(2,1)S(1)} %bitcast.26), channel_id=1, replica_groups=mesh['zh'=4,'zl'=4,'y'=4,'x'=4,'c'=2] {'zl','y','c'}, dimensions={0} | all-to-all | bytes 262144 | tf_op jit(solution)/shard_map/all_to_all | solution.py:36
  94.5 0.6 fusion
  (7 shorter events, 0.1 us)
Async XLA Ops:
  2.0 22.2 %all-to-all-start = ((bf16[8,16,256]{2,1,0:T(8,128)(2,1)}), bf16[8,16,256]{2,1,0:T(8,128)(2,1)S(1)}, u32[]{:S(2)}, u32[]{:S(2)}) async-start(bf16[8,16,256]{2,1,0:T(8,128)(2,1)} %broadcast_in_dim.6), calls=%async_computation | async-start | bytes 131072 | tf_op jit(solution)/shard_map/all_to_all | solution.py:36
  14.0 37.6 %collective-permute-start.1 = (bf16[2,128,256]{2,1,0:T(8,128)(2,1)S(1)}, bf16[2,128,256]{2,1,0:T(8,128)(2,1)S(1)}, u32[]{:S(2)}, u32[]{:S(2)}) collective-permute-start(bf16[2,128,256]{2,1,0:T(8,128)(2,1)S(1)} %get-tuple-element.32.own0), channel_id=1, source_target_pairs={{0,384},{1,129},{128,0},{129,257},{256,128},{257,385},{384,256},{3... | collective-permute-start | bytes 393224 | tf_op jit(solution)/shard_map/ppermute | solution.py:32
  18.6 25.5 %collective-permute-start = (bf16[2,128,256]{2,1,0:T(8,128)(2,1)S(1)}, bf16[2,128,256]{2,1,0:T(8,128)(2,1)S(1)}, u32[]{:S(2)}, u32[]{:S(2)}) collective-permute-start(bf16[2,128,256]{2,1,0:T(8,128)(2,1)S(1)} %get-tuple-element.32.own0), channel_id=1, source_target_pairs={{0,128},{1,385},{128,256},{129,1},{256,384},{257,129},{384,0},{385... | collective-permute-start | bytes 393224 | tf_op jit(solution)/shard_map/ppermute | solution.py:32
  26.7 10.1 %all-to-all-start.1 = ((bf16[8,16,128]{2,1,0:T(8,128)(2,1)}), bf16[8,16,128]{2,1,0:T(8,128)(2,1)S(1)}, u32[]{:S(2)}, u32[]{:S(2)}) async-start(bf16[8,16,128]{2,1,0:T(8,128)(2,1)} %get-tuple-element.28), calls=%async_computation.1 | async-start | bytes 65536 | tf_op jit(solution)/shard_map/all_to_all | solution.py:36
  31.8 5.0 %copy-start = (bf16[16,256]{1,0:T(8,128)(2,1)S(1)}, bf16[16,256]{1,0:T(8,128)(2,1)}, u32[]{:S(2)}) copy-start(bf16[16,256]{1,0:T(8,128)(2,1)} %tokens_ref.1) | copy-start | bytes 24580
  37.6 23.6 %all-to-all-start.2 = ((bf16[32,8,256]{2,1,0:T(8,128)(2,1)}), bf16[32,8,256]{2,1,0:T(8,128)(2,1)S(1)}, u32[]{:S(2)}, u32[]{:S(2)}) async-start(bf16[32,8,256]{2,1,0:T(8,128)(2,1)} %bitcast.8), calls=%async_computation.2 | async-start | bytes 262144 | tf_op jit(solution)/shard_map/all_to_all | solution.py:36
  44.1 13.7 %collective-permute-start.2 = (bf16[2,128,256]{2,1,0:T(8,128)(2,1)S(1)}, bf16[2,128,256]{2,1,0:T(8,128)(2,1)S(1)}, u32[]{:S(2)}, u32[]{:S(2)}) collective-permute-start(bf16[2,128,256]{2,1,0:T(8,128)(2,1)S(1)} %collective-permute-done.own1), channel_id=1, source_target_pairs={{0,128},{1,385},{128,256},{129,1},{256,384},{257,129},{384,0},{385... | collective-permute-start | bytes 393224 | tf_op jit(solution)/shard_map/ppermute | solution.py:32
  57.8 3.4 %collective-permute-start.3 = (bf16[4,128,256]{2,1,0:T(8,128)(2,1)S(1)}, bf16[4,128,256]{2,1,0:T(8,128)(2,1)S(1)}, u32[]{:S(2)}, u32[]{:S(2)}) collective-permute-start(bf16[4,128,256]{2,1,0:T(8,128)(2,1)S(1)} %pad_maximum_fusion), channel_id=1, source_target_pairs={{0,1},{1,0},{2,3},{3,2},{4,5},{5,4},{6,7},{7,6},{8,9},{9,8},{10,11... | collective-permute-start | bytes 786440 | tf_op jit(solution)/shard_map/ppermute | solution.py:23
  62.4 5.8 %copy-start.1 = (f32[16,1,128,128]{3,2,1,0:T(8,128)S(1)}, f32[16,1,128,128]{3,2,1,0:T(8,128)}, u32[]{:S(2)}) copy-start(f32[16,1,128,128]{3,2,1,0:T(8,128)} %param.23) | copy-start | bytes 3145732
  62.4 13.7 %all-to-all-start.3 = ((bf16[4,144,512]{2,1,0:T(8,128)(2,1)}), bf16[4,144,512]{2,1,0:T(8,128)(2,1)S(1)}, u32[]{:S(2)}, u32[]{:S(2)}) async-start(bf16[4,144,512]{2,1,0:T(8,128)(2,1)} %shard_map.177), calls=%async_computation.3 | async-start | bytes 1179648 | tf_op jit(solution)/shard_map/all_to_all | solution.py:36
  66.2 3.4 %collective-permute-start.4 = (bf16[4,128,256]{2,1,0:T(8,128)(2,1)S(1)}, bf16[4,128,256]{2,1,0:T(8,128)(2,1)S(1)}, u32[]{:S(2)}, u32[]{:S(2)}) collective-permute-start(bf16[4,128,256]{2,1,0:T(8,128)(2,1)S(1)} %pad_maximum_fusion.1), channel_id=1, source_target_pairs={{0,1},{1,0},{2,3},{3,2},{4,5},{5,4},{6,7},{7,6},{8,9},{9,8},{10,11... | collective-permute-start | bytes 786440 | tf_op jit(solution)/shard_map/ppermute | solution.py:23

commit v5 on v4

--- a/solution.py
+++ b/solution.py
@@ -253,7 +253,7 @@
         )
     first = mine.astype(f32)
     second = theirs.astype(f32)
-    ones = jnp.ones((16, columns), f32)
+    ones = jnp.ones((8, columns), f32)
     squares = matmul_rows(ones, first * first + second * second, lax.Precision.HIGHEST)
     high = squares.astype(bf16)
     low = (squares - high.astype(f32)).astype(bf16)
@@ -263,7 +263,7 @@
         out_ref[copy, count:, :count] = high
         out_ref[copy, count:, count : 2 * count] = low
         out_ref[copy, count:, 2 * count :] = jnp.zeros(
-            (16, out_ref.shape[2] - 2 * count), bf16
+            (8, out_ref.shape[2] - 2 * count), bf16
         )
 
 
@@ -396,7 +396,7 @@
     count = groups * share
     hidden = down_weight.shape[0] * up_other.shape[0]
     sums = call(
-        up, shape((lax.axis_size("x"), count + 16, hidden), bf16), [SMEM] + [VMEM] * 6
+        up, shape((lax.axis_size("x"), count + 8, hidden), bf16), [SMEM] + [VMEM] * 6
     )(core, rows.reshape(groups, cores, share, columns), *own, up_other)
     sums = exchanged(sums, "x")
     back = call(down, shape((groups, cores, share, columns), bf16), [SMEM] + [VMEM] * 6)(

time: 95.8 us -> 95.4 us (level)
  no operation moved by 1% of the time
where the time goes in v5:
time: 95.4 us; the launch traced here: 94.8 us
  starting transfers between devices  46.8 us (49%)
  waiting for transfers between devices  18.8 us (20%)
  blocking collectives  17.9 us (19%)
  Pallas kernels  6.96 us (7%)
  other arithmetic  2.14 us (2%)
  local copies, waits for them, and re-layouts  1.38 us (1%)
    all_to_all x4, starting transfers between devices, exchanged(): return lax.all_to_all(array, axes, 0, 0, tiled=True)  25.2 us
    all_to_all x1, blocking collectives, exchanged(): return lax.all_to_all(array, axes, 0, 0, tiled=True)  17.9 us
    ppermute x3, starting transfers between devices, crossed(): return lax.ppermute(array, ('zh', 'c'), pairs)  17.6 us
    all_to_all x4, waiting for transfers between devices, exchanged(): return lax.all_to_all(array, axes, 0, 0, tiled=True)  11.2 us
    ppermute x3, waiting for transfers between devices, crossed(): return lax.ppermute(array, ('zh', 'c'), pairs)  6.06 us
    ppermute x2, starting transfers between devices, shifted(): lax.ppermute(array, axis, [(i, (i + step) % size) for i in range(size)])  3.96 us
    pallas_call x1, Pallas kernels, body(): call(cell, (shape((parts, sequences, dim), bf16), shape((sequences, dim),...  2.52 us
    pallas_call x1, Pallas kernels, body(): call(prepare, tuple((shape(array.shape, array.dtype) for array in fetched...  1.98 us
  transfers between devices with their start and end apart: 9, of which 4 were waited for; matrix products, arithmetic and copies ran while one was open for 2% of the time, Pallas kernels for 6%

profile of v5, /device:TPU:1, one launch (start us, length us, event | category | flops | bytes accessed | tf_op | source)
XLA Modules:
  0.0 94.8 jit_solution(15075249281924218948)
XLA Ops:
  0.6 1.3 %broadcast_in_dim.6 = bf16[8,16,256]{2,1,0:T(8,128)(2,1)} broadcast(bf16[16,256]{1,0:T(8,128)(2,1)} %tokens_ref.1), dimensions={1,2} | broadcast | bytes 73728 | tf_op jit(solution)/shard_map/broadcast_in_dim | solution.py:328
  2.0 10.1 %all-to-all-start = ((bf16[8,16,256]{2,1,0:T(8,128)(2,1)}), bf16[8,16,256]{2,1,0:T(8,128)(2,1)S(1)}, u32[]{:S(2)}, u32[]{:S(2)}) async-start(bf16[8,16,256]{2,1,0:T(8,128)(2,1)} %broadcast_in_dim.6), calls=%async_computation | async-start | bytes 131072 | tf_op jit(solution)/shard_map/all_to_all | solution.py:36
  12.1 2.0 %shard_map.174 = (bf16[2048,128]{1,0:T(8,128)(2,1)S(1)}, bf16[2048,128]{1,0:T(8,128)(2,1)S(1)}, bf16[2048,128]{1,0:T(8,128)(2,1)S(1)}, bf16[2048,128]{1,0:T(8,12...) custom-call(s32[1]{0:T(128)} %bitcast.head_ref, ...), custom_call_target="tpu_custom_call" | custom-call | flops 1000000 | bytes 1000000 | tf_op jit(solution)/shard_map/pallas_call | solution.py:341
  14.0 4.5 %collective-permute-start.1 = (bf16[2,128,256]{2,1,0:T(8,128)(2,1)S(1)}, bf16[2,128,256]{2,1,0:T(8,128)(2,1)S(1)}, u32[]{:S(2)}, u32[]{:S(2)}) collective-permute-start(bf16[2,128,256]{2,1,0:T(8,128)(2,1)S(1)} %get-tuple-element.32.own0), channel_id=1, source_target_pairs={{0,384},{1,129},{128,0},{129,257},{256,128},{257,385},{384,256},{3... | collective-permute-start | bytes 393224 | tf_op jit(solution)/shard_map/ppermute | solution.py:32
  18.6 5.6 %collective-permute-start = (bf16[2,128,256]{2,1,0:T(8,128)(2,1)S(1)}, bf16[2,128,256]{2,1,0:T(8,128)(2,1)S(1)}, u32[]{:S(2)}, u32[]{:S(2)}) collective-permute-start(bf16[2,128,256]{2,1,0:T(8,128)(2,1)S(1)} %get-tuple-element.32.own0), channel_id=1, source_target_pairs={{0,128},{1,385},{128,256},{129,1},{256,384},{257,129},{384,0},{385... | collective-permute-start | bytes 393224 | tf_op jit(solution)/shard_map/ppermute | solution.py:32
  24.1 0.0 all-to-all-done.tiles_ref
  24.1 2.5 %shard_map.175 = (bf16[8,16,128]{2,1,0:T(8,128)(2,1)}, f32[16,128]{1,0:T(8,128)}, f32[1,16]{1,0:T(1,128)}, f32[16,1]{1,0:T(8,128)S(1)}, f32[16,128]{1,0:T(8,128)S(1)}, /*index=5*/f32[16,128]{1,0:T(8,128)S(1)}) custom-call(bf16[8,16,256]{2,1,0:T(8,128)(2,1)S(1)} %all-to-all-done.tiles_ref, bf16[2048,128]{1,0:T(8,128)(2,1)S(1)} %get-tuple-element.22.query_ref, ...), custom_call_target="tpu_custom_call" | custom-call | flops 1000000 | bytes 1000000 | tf_op jit(solution)/shard_map/pallas_call | solution.py:363
  26.7 5.1 %all-to-all-start.1 = ((bf16[8,16,128]{2,1,0:T(8,128)(2,1)}), bf16[8,16,128]{2,1,0:T(8,128)(2,1)S(1)}, u32[]{:S(2)}, u32[]{:S(2)}) async-start(bf16[8,16,128]{2,1,0:T(8,128)(2,1)} %get-tuple-element.28), calls=%async_computation.1 | async-start | bytes 65536 | tf_op jit(solution)/shard_map/all_to_all | solution.py:36
  31.8 0.0 copy-start
  31.8 5.0 %all-to-all-done.1.tiles_ref = bf16[8,16,128]{2,1,0:T(8,128)(2,1)S(1)} async-done(((bf16[8,16,128]{2,1,0:T(8,128)(2,1)}), bf16[8,16,128]{2,1,0:T(8,128)(2,1)S(1)}, u32[]{:S(2)}, u32[]{:S(2)}) %all-to-all-start.1) | async-done | bytes 32800 | tf_op jit(solution)/shard_map/all_to_all | solution.py:36
  36.8 0.0 copy-done
  36.8 0.8 shard_map.176
  37.6 6.4 %all-to-all-start.2 = ((bf16[32,8,256]{2,1,0:T(8,128)(2,1)}), bf16[32,8,256]{2,1,0:T(8,128)(2,1)S(1)}, u32[]{:S(2)}, u32[]{:S(2)}) async-start(bf16[32,8,256]{2,1,0:T(8,128)(2,1)} %bitcast.8), calls=%async_computation.2 | async-start | bytes 262144 | tf_op jit(solution)/shard_map/all_to_all | solution.py:36
  44.1 0.0 collective-permute-done.own1
  44.1 7.5 %collective-permute-start.2 = (bf16[2,128,256]{2,1,0:T(8,128)(2,1)S(1)}, bf16[2,128,256]{2,1,0:T(8,128)(2,1)S(1)}, u32[]{:S(2)}, u32[]{:S(2)}) collective-permute-start(bf16[2,128,256]{2,1,0:T(8,128)(2,1)S(1)} %collective-permute-done.own1), channel_id=1, source_target_pairs={{0,128},{1,385},{128,256},{129,1},{256,384},{257,129},{384,0},{385... | collective-permute-start | bytes 393224 | tf_op jit(solution)/shard_map/ppermute | solution.py:32
  51.6 0.0 collective-permute-done.1.own2
  51.7 6.1 %collective-permute-done.2.own3 = bf16[2,128,256]{2,1,0:T(8,128)(2,1)S(1)} collective-permute-done((bf16[2,128,256]{2,1,0:T(8,128)(2,1)S(1)}, bf16[2,128,256]{2,1,0:T(8,128)(2,1)S(1)}, u32[]{:S(2)}, u32[]{:S(2)}) %collective-permute-start.2) | collective-permute-done | bytes 131104 | tf_op jit(solution)/shard_map/ppermute | solution.py:32
  57.8 1.9 %collective-permute-start.3 = (bf16[4,128,256]{2,1,0:T(8,128)(2,1)S(1)}, bf16[4,128,256]{2,1,0:T(8,128)(2,1)S(1)}, u32[]{:S(2)}, u32[]{:S(2)}) collective-permute-start(bf16[4,128,256]{2,1,0:T(8,128)(2,1)S(1)} %pad_maximum_fusion), channel_id=1, source_target_pairs={{0,1},{1,0},{2,3},{3,2},{4,5},{5,4},{6,7},{7,6},{8,9},{9,8},{10,11... | collective-permute-start | bytes 786440 | tf_op jit(solution)/shard_map/ppermute | solution.py:23
  59.7 1.5 %collective-permute-done.3.other_ref = bf16[4,128,256]{2,1,0:T(8,128)(2,1)S(1)} collective-permute-done((bf16[4,128,256]{2,1,0:T(8,128)(2,1)S(1)}, bf16[4,128,256]{2,1,0:T(8,128)(2,1)S(1)}, u32[]{:S(2)}, u32[]{:S(2)}) %collective-permute-start.3) | collective-permute-done | bytes 262176 | tf_op jit(solution)/shard_map/ppermute | solution.py:23
  61.2 0.0 all-to-all-done.2
  61.2 1.2 %shard_map.177 = bf16[4,136,512]{2,1,0:T(8,128)(2,1)} custom-call(s32[1]{0:T(128)} %bitcast.7.core_ref, bf16[16,2,8,256]{3,2,1,0:T(8,128)(2,1)S(1)} %bitcast.25, bf16[2,128,256]{2,1,0:T(8,128)(2,1)S(1)} %get-tuple-element.32.own0, bf16[2,128,256]{2,1,0:T(8,128)(2,1)S(1)} %collective-permute-done.own1, bf16[2,128,256]{2,1,0:T(8,128)(2,1)S(1)} %collective-permute-done.1.own2, ...), custom_call_target="tpu_custom_call" | custom-call | flops 1000000 | bytes 1000000 | tf_op jit(solution)/shard_map/pallas_call | solution.py:398
  62.4 0.0 copy-start.1
  62.4 3.6 %all-to-all-start.3 = ((bf16[4,136,512]{2,1,0:T(8,128)(2,1)}), bf16[4,136,512]{2,1,0:T(8,128)(2,1)S(1)}, u32[]{:S(2)}, u32[]{:S(2)}) async-start(bf16[4,136,512]{2,1,0:T(8,128)(2,1)} %shard_map.177), calls=%async_computation.3 | async-start | bytes 1114112 | tf_op jit(solution)/shard_map/all_to_all | solution.py:36
  66.0 0.1 reduce
  66.2 2.0 %collective-permute-start.4 = (bf16[4,128,256]{2,1,0:T(8,128)(2,1)S(1)}, bf16[4,128,256]{2,1,0:T(8,128)(2,1)S(1)}, u32[]{:S(2)}, u32[]{:S(2)}) collective-permute-start(bf16[4,128,256]{2,1,0:T(8,128)(2,1)S(1)} %pad_maximum_fusion.1), channel_id=1, source_target_pairs={{0,1},{1,0},{2,3},{3,2},{4,5},{5,4},{6,7},{7,6},{8,9},{9,8},{10,11... | collective-permute-start | bytes 786440 | tf_op jit(solution)/shard_map/ppermute | solution.py:23
  68.2 0.0 copy-done.1
  68.3 1.3 %multiply_add_fusion = f32[16,128,128]{2,1,0:T(8,128)} fusion(f32[16,128]{1,0:T(8,128)S(1)} %get-tuple-element.35, f32[16,128]{1,0:T(8,128)S(1)} %get-tuple-element.34, f32[16]{0:T(128)S(1)} %reduce, f32[16,1,128,128]{3,2,1,0:T(8,128)S(1)} %copy-done.1), kind=kLoop, calls=%fused_computation | loop fusion | flops 786432 | bytes 2113600 | tf_op jit(solution)/shard_map/add | solution.py:383
  69.6 0.0 collective-permute-done.4.other_ref
  69.6 6.2 %all-to-all-done.3.sums_ref = bf16[4,136,512]{2,1,0:T(8,128)(2,1)S(1)} async-done(((bf16[4,136,512]{2,1,0:T(8,128)(2,1)}), bf16[4,136,512]{2,1,0:T(8,128)(2,1)S(1)}, u32[]{:S(2)}, u32[]{:S(2)}) %all-to-all-start.3) | async-done | bytes 557088 | tf_op jit(solution)/shard_map/all_to_all | solution.py:36
  75.8 0.4 shard_map.178
  76.2 17.9 %all_to_all.25 = bf16[32,8,256]{2,1,0:T(8,128)(2,1)S(1)} all-to-all(bf16[32,8,256]{2,1,0:T(8,128)(2,1)S(1)} %bitcast.26), channel_id=1, replica_groups=mesh['zh'=4,'zl'=4,'y'=4,'x'=4,'c'=2] {'zl','y','c'}, dimensions={0} | all-to-all | bytes 262144 | tf_op jit(solution)/shard_map/all_to_all | solution.py:36
  94.2 0.6 fusion
  (7 shorter events, 0.1 us)
Async XLA Ops:
  2.0 22.2 %all-to-all-start = ((bf16[8,16,256]{2,1,0:T(8,128)(2,1)}), bf16[8,16,256]{2,1,0:T(8,128)(2,1)S(1)}, u32[]{:S(2)}, u32[]{:S(2)}) async-start(bf16[8,16,256]{2,1,0:T(8,128)(2,1)} %broadcast_in_dim.6), calls=%async_computation | async-start | bytes 131072 | tf_op jit(solution)/shard_map/all_to_all | solution.py:36
  14.0 37.6 %collective-permute-start.1 = (bf16[2,128,256]{2,1,0:T(8,128)(2,1)S(1)}, bf16[2,128,256]{2,1,0:T(8,128)(2,1)S(1)}, u32[]{:S(2)}, u32[]{:S(2)}) collective-permute-start(bf16[2,128,256]{2,1,0:T(8,128)(2,1)S(1)} %get-tuple-element.32.own0), channel_id=1, source_target_pairs={{0,384},{1,129},{128,0},{129,257},{256,128},{257,385},{384,256},{3... | collective-permute-start | bytes 393224 | tf_op jit(solution)/shard_map/ppermute | solution.py:32
  18.6 25.5 %collective-permute-start = (bf16[2,128,256]{2,1,0:T(8,128)(2,1)S(1)}, bf16[2,128,256]{2,1,0:T(8,128)(2,1)S(1)}, u32[]{:S(2)}, u32[]{:S(2)}) collective-permute-start(bf16[2,128,256]{2,1,0:T(8,128)(2,1)S(1)} %get-tuple-element.32.own0), channel_id=1, source_target_pairs={{0,128},{1,385},{128,256},{129,1},{256,384},{257,129},{384,0},{385... | collective-permute-start | bytes 393224 | tf_op jit(solution)/shard_map/ppermute | solution.py:32
  26.7 10.1 %all-to-all-start.1 = ((bf16[8,16,128]{2,1,0:T(8,128)(2,1)}), bf16[8,16,128]{2,1,0:T(8,128)(2,1)S(1)}, u32[]{:S(2)}, u32[]{:S(2)}) async-start(bf16[8,16,128]{2,1,0:T(8,128)(2,1)} %get-tuple-element.28), calls=%async_computation.1 | async-start | bytes 65536 | tf_op jit(solution)/shard_map/all_to_all | solution.py:36
  31.8 5.0 %copy-start = (bf16[16,256]{1,0:T(8,128)(2,1)S(1)}, bf16[16,256]{1,0:T(8,128)(2,1)}, u32[]{:S(2)}) copy-start(bf16[16,256]{1,0:T(8,128)(2,1)} %tokens_ref.1) | copy-start | bytes 24580
  37.6 23.6 %all-to-all-start.2 = ((bf16[32,8,256]{2,1,0:T(8,128)(2,1)}), bf16[32,8,256]{2,1,0:T(8,128)(2,1)S(1)}, u32[]{:S(2)}, u32[]{:S(2)}) async-start(bf16[32,8,256]{2,1,0:T(8,128)(2,1)} %bitcast.8), calls=%async_computation.2 | async-start | bytes 262144 | tf_op jit(solution)/shard_map/all_to_all | solution.py:36
  44.1 13.7 %collective-permute-start.2 = (bf16[2,128,256]{2,1,0:T(8,128)(2,1)S(1)}, bf16[2,128,256]{2,1,0:T(8,128)(2,1)S(1)}, u32[]{:S(2)}, u32[]{:S(2)}) collective-permute-start(bf16[2,128,256]{2,1,0:T(8,128)(2,1)S(1)} %collective-permute-done.own1), channel_id=1, source_target_pairs={{0,128},{1,385},{128,256},{129,1},{256,384},{257,129},{384,0},{385... | collective-permute-start | bytes 393224 | tf_op jit(solution)/shard_map/ppermute | solution.py:32
  57.8 3.4 %collective-permute-start.3 = (bf16[4,128,256]{2,1,0:T(8,128)(2,1)S(1)}, bf16[4,128,256]{2,1,0:T(8,128)(2,1)S(1)}, u32[]{:S(2)}, u32[]{:S(2)}) collective-permute-start(bf16[4,128,256]{2,1,0:T(8,128)(2,1)S(1)} %pad_maximum_fusion), channel_id=1, source_target_pairs={{0,1},{1,0},{2,3},{3,2},{4,5},{5,4},{6,7},{7,6},{8,9},{9,8},{10,11... | collective-permute-start | bytes 786440 | tf_op jit(solution)/shard_map/ppermute | solution.py:23
  62.4 5.8 %copy-start.1 = (f32[16,1,128,128]{3,2,1,0:T(8,128)S(1)}, f32[16,1,128,128]{3,2,1,0:T(8,128)}, u32[]{:S(2)}) copy-start(f32[16,1,128,128]{3,2,1,0:T(8,128)} %param.23) | copy-start | bytes 3145732
  62.4 13.4 %all-to-all-start.3 = ((bf16[4,136,512]{2,1,0:T(8,128)(2,1)}), bf16[4,136,512]{2,1,0:T(8,128)(2,1)S(1)}, u32[]{:S(2)}, u32[]{:S(2)}) async-start(bf16[4,136,512]{2,1,0:T(8,128)(2,1)} %shard_map.177), calls=%async_computation.3 | async-start | bytes 1114112 | tf_op jit(solution)/shard_map/all_to_all | solution.py:36
  66.2 3.4 %collective-permute-start.4 = (bf16[4,128,256]{2,1,0:T(8,128)(2,1)S(1)}, bf16[4,128,256]{2,1,0:T(8,128)(2,1)S(1)}, u32[]{:S(2)}, u32[]{:S(2)}) collective-permute-start(bf16[4,128,256]{2,1,0:T(8,128)(2,1)S(1)} %pad_maximum_fusion.1), channel_id=1, source_target_pairs={{0,1},{1,0},{2,3},{3,2},{4,5},{5,4},{6,7},{7,6},{8,9},{9,8},{10,11... | collective-permute-start | bytes 786440 | tf_op jit(solution)/shard_map/ppermute | solution.py:23

commit v6 on v5

--- a/solution.py
+++ b/solution.py
@@ -61,11 +61,13 @@
     value_source,
     outgate_source,
     out_source,
+    state_source,
     query_ref,
     key_ref,
     value_ref,
     outgate_ref,
     out_ref,
+    first_ref,
     gates_ref,
     small_ref,
     block_ref,
@@ -93,6 +95,7 @@
         (value_source, value_ref),
         (outgate_source, outgate_ref),
         (out_source, out_ref),
+        (state_source.at[pl.ds(0, first_ref.shape[0])], first_ref),
     )
     copies = [
         pltpu.make_async_copy(source, target, semaphores.at[index])
@@ -138,6 +141,7 @@
     value_ref,
     outgate_ref,
     state_source,
+    first_ref,
     gates_ref,
     small_ref,
     mixed_ref,
@@ -149,10 +153,11 @@
     state_ref,
     semaphores,
 ):
+    half = first_ref.shape[0]
     step = state_ref.shape[0] // semaphores.shape[0]
     fetches = [
         pltpu.make_async_copy(
-            state_source.at[pl.ds(index * step, step)],
+            state_source.at[pl.ds(half + index * step, step)],
             state_ref.at[pl.ds(index * step, step)],
             semaphores.at[index],
         )
@@ -214,7 +219,11 @@
         fetch.wait()
     read = jnp.concatenate(
         [
-            jnp.sum(columns[:, s : s + 1] * state_ref[s], axis=0, keepdims=True)
+            jnp.sum(
+                columns[:, s : s + 1] * (first_ref[s] if s < half else state_ref[s - half]),
+                axis=0,
+                keepdims=True,
+            )
             for s in range(sequences)
         ],
         axis=0,
@@ -337,10 +346,11 @@
         state_max.reshape(1, -1),
         forget_bias.reshape(1, -1),
     )
-    fetched = (query_weight, key_weight, value_weight, outgate_weight, out_weight)
-    *projections, out_weight, gates, small, block = call(
+    fetched = (query_weight, key_weight, value_weight, outgate_weight, out_weight, state_matrix[:, 0])
+    *projections, out_weight, first_state, gates, small, block = call(
         prepare,
-        tuple(shape(array.shape, array.dtype) for array in fetched)
+        tuple(shape(array.shape, array.dtype) for array in fetched[:5])
+        + (shape((sequences // 4, dim, dim), f32),)
         + (
             shape((2, attn_gain.shape[0]), f32),
             shape((attn_gain.shape[0] // dim + sequences + 8, dim), f32),
@@ -370,12 +380,13 @@
             shape((sequences, dim), f32),
             shape((sequences, dim), f32),
         ),
-        [VMEM] * 5 + [HBM] + [VMEM] * 2,
-        scratch=[pltpu.VMEM((sequences, dim, dim), f32), pltpu.SemaphoreType.DMA((4,))],
+        [VMEM] * 5 + [HBM] + [VMEM] * 3,
+        scratch=[pltpu.VMEM((sequences - sequences // 4, dim, dim), f32), pltpu.SemaphoreType.DMA((4,))],
     )(
         tiles,
         *projections,
         pltpu.with_memory_space_constraint(state_matrix[:, 0], pltpu.HBM),
+        first_state,
         gates,
         small,
     )

time: 95.4 us -> 95.5 us (level)
  no operation moved by 1% of the time
where the time goes in v6:
time: 95.5 us; the launch traced here: 94.9 us
  starting transfers between devices  46.8 us (49%)
  waiting for transfers between devices  18.8 us (20%)
  blocking collectives  17.9 us (19%)
  Pallas kernels  7.07 us (7%)
  other arithmetic  2.14 us (2%)
  local copies, waits for them, and re-layouts  1.38 us (1%)
    all_to_all x4, starting transfers between devices, exchanged(): return lax.all_to_all(array, axes, 0, 0, tiled=True)  25.2 us
    all_to_all x1, blocking collectives, exchanged(): return lax.all_to_all(array, axes, 0, 0, tiled=True)  17.9 us
    ppermute x3, starting transfers between devices, crossed(): return lax.ppermute(array, ('zh', 'c'), pairs)  17.6 us
    all_to_all x4, waiting for transfers between devices, exchanged(): return lax.all_to_all(array, axes, 0, 0, tiled=True)  11.2 us
    ppermute x3, waiting for transfers between devices, crossed(): return lax.ppermute(array, ('zh', 'c'), pairs)  6.06 us
    ppermute x2, starting transfers between devices, shifted(): lax.ppermute(array, axis, [(i, (i + step) % size) for i in range(size)])  3.97 us
    pallas_call x1, Pallas kernels, body(): call(cell, (shape((parts, sequences, dim), bf16), shape((sequences, dim),...  2.55 us
    pallas_call x1, Pallas kernels, body(): call(prepare, tuple((shape(array.shape, array.dtype) for array in fetched...  2.05 us
  transfers between devices with their start and end apart: 9, of which 4 were waited for; matrix products, arithmetic and copies ran while one was open for 2% of the time, Pallas kernels for 6%

profile of v6, /device:TPU:1, one launch (start us, length us, event | category | flops | bytes accessed | tf_op | source)
XLA Modules:
  0.0 94.9 jit_solution(9934418956688160309)
XLA Ops:
  0.6 1.3 %broadcast_in_dim.6 = bf16[8,16,256]{2,1,0:T(8,128)(2,1)} broadcast(bf16[16,256]{1,0:T(8,128)(2,1)} %tokens_ref.1), dimensions={1,2} | broadcast | bytes 73728 | tf_op jit(solution)/shard_map/broadcast_in_dim | solution.py:337
  2.0 10.1 %all-to-all-start = ((bf16[8,16,256]{2,1,0:T(8,128)(2,1)}), bf16[8,16,256]{2,1,0:T(8,128)(2,1)S(1)}, u32[]{:S(2)}, u32[]{:S(2)}) async-start(bf16[8,16,256]{2,1,0:T(8,128)(2,1)} %broadcast_in_dim.6), calls=%async_computation | async-start | bytes 131072 | tf_op jit(solution)/shard_map/all_to_all | solution.py:36
  12.1 2.0 %shard_map.174 = (bf16[2048,128]{1,0:T(8,128)(2,1)S(1)}, bf16[2048,128]{1,0:T(8,128)(2,1)S(1)}, bf16[2048,128]{1,0:T(8,128)(2,1)S(1)}, bf16[2048,128]{1,0:T(8,12...) custom-call(s32[1]{0:T(128)} %bitcast.head_ref, ...), custom_call_target="tpu_custom_call" | custom-call | flops 1000000 | bytes 1000000 | tf_op jit(solution)/shard_map/pallas_call | solution.py:350
  14.1 4.5 %collective-permute-start.1 = (bf16[2,128,256]{2,1,0:T(8,128)(2,1)S(1)}, bf16[2,128,256]{2,1,0:T(8,128)(2,1)S(1)}, u32[]{:S(2)}, u32[]{:S(2)}) collective-permute-start(bf16[2,128,256]{2,1,0:T(8,128)(2,1)S(1)} %get-tuple-element.34.own0), channel_id=1, source_target_pairs={{0,384},{1,129},{128,0},{129,257},{256,128},{257,385},{384,256},{3... | collective-permute-start | bytes 393224 | tf_op jit(solution)/shard_map/ppermute | solution.py:32
  18.6 5.6 %collective-permute-start = (bf16[2,128,256]{2,1,0:T(8,128)(2,1)S(1)}, bf16[2,128,256]{2,1,0:T(8,128)(2,1)S(1)}, u32[]{:S(2)}, u32[]{:S(2)}) collective-permute-start(bf16[2,128,256]{2,1,0:T(8,128)(2,1)S(1)} %get-tuple-element.34.own0), channel_id=1, source_target_pairs={{0,128},{1,385},{128,256},{129,1},{256,384},{257,129},{384,0},{385... | collective-permute-start | bytes 393224 | tf_op jit(solution)/shard_map/ppermute | solution.py:32
  24.2 0.0 all-to-all-done.tiles_ref
  24.2 2.5 %shard_map.175 = (bf16[8,16,128]{2,1,0:T(8,128)(2,1)}, f32[16,128]{1,0:T(8,128)}, f32[1,16]{1,0:T(1,128)}, f32[16,1]{1,0:T(8,128)S(1)}, f32[16,128]{1,0:T(8,128)S(1)}, /*index=5*/f32[16,128]{1,0:T(8,128)S(1)}) custom-call(bf16[8,16,256]{2,1,0:T(8,128)(2,1)S(1)} %all-to-all-done.tiles_ref, bf16[2048,128]{1,0:T(8,128)(2,1)S(1)} %get-tuple-element.23.query_ref, ...), custom_call_target="tpu_custom_call" | custom-call | flops 1000000 | bytes 1000000 | tf_op jit(solution)/shard_map/pallas_call | solution.py:373
  26.8 5.1 %all-to-all-start.1 = ((bf16[8,16,128]{2,1,0:T(8,128)(2,1)}), bf16[8,16,128]{2,1,0:T(8,128)(2,1)S(1)}, u32[]{:S(2)}, u32[]{:S(2)}) async-start(bf16[8,16,128]{2,1,0:T(8,128)(2,1)} %get-tuple-element.30), calls=%async_computation.1 | async-start | bytes 65536 | tf_op jit(solution)/shard_map/all_to_all | solution.py:36
  31.9 0.0 copy-start
  31.9 5.0 %all-to-all-done.1.tiles_ref = bf16[8,16,128]{2,1,0:T(8,128)(2,1)S(1)} async-done(((bf16[8,16,128]{2,1,0:T(8,128)(2,1)}), bf16[8,16,128]{2,1,0:T(8,128)(2,1)S(1)}, u32[]{:S(2)}, u32[]{:S(2)}) %all-to-all-start.1) | async-done | bytes 32800 | tf_op jit(solution)/shard_map/all_to_all | solution.py:36
  36.9 0.0 copy-done
  36.9 0.8 shard_map.176
  37.7 6.4 %all-to-all-start.2 = ((bf16[32,8,256]{2,1,0:T(8,128)(2,1)}), bf16[32,8,256]{2,1,0:T(8,128)(2,1)S(1)}, u32[]{:S(2)}, u32[]{:S(2)}) async-start(bf16[32,8,256]{2,1,0:T(8,128)(2,1)} %bitcast.8), calls=%async_computation.2 | async-start | bytes 262144 | tf_op jit(solution)/shard_map/all_to_all | solution.py:36
  44.2 0.0 collective-permute-done.own1
  44.2 7.5 %collective-permute-start.2 = (bf16[2,128,256]{2,1,0:T(8,128)(2,1)S(1)}, bf16[2,128,256]{2,1,0:T(8,128)(2,1)S(1)}, u32[]{:S(2)}, u32[]{:S(2)}) collective-permute-start(bf16[2,128,256]{2,1,0:T(8,128)(2,1)S(1)} %collective-permute-done.own1), channel_id=1, source_target_pairs={{0,128},{1,385},{128,256},{129,1},{256,384},{257,129},{384,0},{385... | collective-permute-start | bytes 393224 | tf_op jit(solution)/shard_map/ppermute | solution.py:32
  51.7 0.0 collective-permute-done.1.own2
  51.8 6.1 %collective-permute-done.2.own3 = bf16[2,128,256]{2,1,0:T(8,128)(2,1)S(1)} collective-permute-done((bf16[2,128,256]{2,1,0:T(8,128)(2,1)S(1)}, bf16[2,128,256]{2,1,0:T(8,128)(2,1)S(1)}, u32[]{:S(2)}, u32[]{:S(2)}) %collective-permute-start.2) | collective-permute-done | bytes 131104 | tf_op jit(solution)/shard_map/ppermute | solution.py:32
  57.9 1.9 %collective-permute-start.3 = (bf16[4,128,256]{2,1,0:T(8,128)(2,1)S(1)}, bf16[4,128,256]{2,1,0:T(8,128)(2,1)S(1)}, u32[]{:S(2)}, u32[]{:S(2)}) collective-permute-start(bf16[4,128,256]{2,1,0:T(8,128)(2,1)S(1)} %pad_maximum_fusion), channel_id=1, source_target_pairs={{0,1},{1,0},{2,3},{3,2},{4,5},{5,4},{6,7},{7,6},{8,9},{9,8},{10,11... | collective-permute-start | bytes 786440 | tf_op jit(solution)/shard_map/ppermute | solution.py:23
  59.8 1.5 %collective-permute-done.3.other_ref = bf16[4,128,256]{2,1,0:T(8,128)(2,1)S(1)} collective-permute-done((bf16[4,128,256]{2,1,0:T(8,128)(2,1)S(1)}, bf16[4,128,256]{2,1,0:T(8,128)(2,1)S(1)}, u32[]{:S(2)}, u32[]{:S(2)}) %collective-permute-start.3) | collective-permute-done | bytes 262176 | tf_op jit(solution)/shard_map/ppermute | solution.py:23
  61.3 0.0 all-to-all-done.2
  61.3 1.2 %shard_map.177 = bf16[4,136,512]{2,1,0:T(8,128)(2,1)} custom-call(s32[1]{0:T(128)} %bitcast.7.core_ref, bf16[16,2,8,256]{3,2,1,0:T(8,128)(2,1)S(1)} %bitcast.25, bf16[2,128,256]{2,1,0:T(8,128)(2,1)S(1)} %get-tuple-element.34.own0, bf16[2,128,256]{2,1,0:T(8,128)(2,1)S(1)} %collective-permute-done.own1, bf16[2,128,256]{2,1,0:T(8,128)(2,1)S(1)} %collective-permute-done.1.own2, ...), custom_call_target="tpu_custom_call" | custom-call | flops 1000000 | bytes 1000000 | tf_op jit(solution)/shard_map/pallas_call | solution.py:409
  62.5 0.0 copy-start.1
  62.5 3.6 %all-to-all-start.3 = ((bf16[4,136,512]{2,1,0:T(8,128)(2,1)}), bf16[4,136,512]{2,1,0:T(8,128)(2,1)S(1)}, u32[]{:S(2)}, u32[]{:S(2)}) async-start(bf16[4,136,512]{2,1,0:T(8,128)(2,1)} %shard_map.177), calls=%async_computation.3 | async-start | bytes 1114112 | tf_op jit(solution)/shard_map/all_to_all | solution.py:36
  66.1 0.1 reduce
  66.3 2.0 %collective-permute-start.4 = (bf16[4,128,256]{2,1,0:T(8,128)(2,1)S(1)}, bf16[4,128,256]{2,1,0:T(8,128)(2,1)S(1)}, u32[]{:S(2)}, u32[]{:S(2)}) collective-permute-start(bf16[4,128,256]{2,1,0:T(8,128)(2,1)S(1)} %pad_maximum_fusion.1), channel_id=1, source_target_pairs={{0,1},{1,0},{2,3},{3,2},{4,5},{5,4},{6,7},{7,6},{8,9},{9,8},{10,11... | collective-permute-start | bytes 786440 | tf_op jit(solution)/shard_map/ppermute | solution.py:23
  68.3 0.0 copy-done.1
  68.4 1.3 %multiply_add_fusion = f32[16,128,128]{2,1,0:T(8,128)} fusion(f32[16,128]{1,0:T(8,128)S(1)} %get-tuple-element.37, f32[16,128]{1,0:T(8,128)S(1)} %get-tuple-element.36, f32[16]{0:T(128)S(1)} %reduce, f32[16,1,128,128]{3,2,1,0:T(8,128)S(1)} %copy-done.1), kind=kLoop, calls=%fused_computation | loop fusion | flops 786432 | bytes 2113600 | tf_op jit(solution)/shard_map/add | solution.py:394
  69.7 0.0 collective-permute-done.4.other_ref
  69.7 6.2 %all-to-all-done.3.sums_ref = bf16[4,136,512]{2,1,0:T(8,128)(2,1)S(1)} async-done(((bf16[4,136,512]{2,1,0:T(8,128)(2,1)}), bf16[4,136,512]{2,1,0:T(8,128)(2,1)S(1)}, u32[]{:S(2)}, u32[]{:S(2)}) %all-to-all-start.3) | async-done | bytes 557088 | tf_op jit(solution)/shard_map/all_to_all | solution.py:36
  75.9 0.4 shard_map.178
  76.3 17.9 %all_to_all.25 = bf16[32,8,256]{2,1,0:T(8,128)(2,1)S(1)} all-to-all(bf16[32,8,256]{2,1,0:T(8,128)(2,1)S(1)} %bitcast.26), channel_id=1, replica_groups=mesh['zh'=4,'zl'=4,'y'=4,'x'=4,'c'=2] {'zl','y','c'}, dimensions={0} | all-to-all | bytes 262144 | tf_op jit(solution)/shard_map/all_to_all | solution.py:36
  94.3 0.6 fusion
  (7 shorter events, 0.1 us)
Async XLA Ops:
  2.0 22.2 %all-to-all-start = ((bf16[8,16,256]{2,1,0:T(8,128)(2,1)}), bf16[8,16,256]{2,1,0:T(8,128)(2,1)S(1)}, u32[]{:S(2)}, u32[]{:S(2)}) async-start(bf16[8,16,256]{2,1,0:T(8,128)(2,1)} %broadcast_in_dim.6), calls=%async_computation | async-start | bytes 131072 | tf_op jit(solution)/shard_map/all_to_all | solution.py:36
  14.1 37.6 %collective-permute-start.1 = (bf16[2,128,256]{2,1,0:T(8,128)(2,1)S(1)}, bf16[2,128,256]{2,1,0:T(8,128)(2,1)S(1)}, u32[]{:S(2)}, u32[]{:S(2)}) collective-permute-start(bf16[2,128,256]{2,1,0:T(8,128)(2,1)S(1)} %get-tuple-element.34.own0), channel_id=1, source_target_pairs={{0,384},{1,129},{128,0},{129,257},{256,128},{257,385},{384,256},{3... | collective-permute-start | bytes 393224 | tf_op jit(solution)/shard_map/ppermute | solution.py:32
  18.6 25.5 %collective-permute-start = (bf16[2,128,256]{2,1,0:T(8,128)(2,1)S(1)}, bf16[2,128,256]{2,1,0:T(8,128)(2,1)S(1)}, u32[]{:S(2)}, u32[]{:S(2)}) collective-permute-start(bf16[2,128,256]{2,1,0:T(8,128)(2,1)S(1)} %get-tuple-element.34.own0), channel_id=1, source_target_pairs={{0,128},{1,385},{128,256},{129,1},{256,384},{257,129},{384,0},{385... | collective-permute-start | bytes 393224 | tf_op jit(solution)/shard_map/ppermute | solution.py:32
  26.8 10.1 %all-to-all-start.1 = ((bf16[8,16,128]{2,1,0:T(8,128)(2,1)}), bf16[8,16,128]{2,1,0:T(8,128)(2,1)S(1)}, u32[]{:S(2)}, u32[]{:S(2)}) async-start(bf16[8,16,128]{2,1,0:T(8,128)(2,1)} %get-tuple-element.30), calls=%async_computation.1 | async-start | bytes 65536 | tf_op jit(solution)/shard_map/all_to_all | solution.py:36
  31.9 5.0 %copy-start = (bf16[16,256]{1,0:T(8,128)(2,1)S(1)}, bf16[16,256]{1,0:T(8,128)(2,1)}, u32[]{:S(2)}) copy-start(bf16[16,256]{1,0:T(8,128)(2,1)} %tokens_ref.1) | copy-start | bytes 24580
  37.7 23.6 %all-to-all-start.2 = ((bf16[32,8,256]{2,1,0:T(8,128)(2,1)}), bf16[32,8,256]{2,1,0:T(8,128)(2,1)S(1)}, u32[]{:S(2)}, u32[]{:S(2)}) async-start(bf16[32,8,256]{2,1,0:T(8,128)(2,1)} %bitcast.8), calls=%async_computation.2 | async-start | bytes 262144 | tf_op jit(solution)/shard_map/all_to_all | solution.py:36
  44.2 13.7 %collective-permute-start.2 = (bf16[2,128,256]{2,1,0:T(8,128)(2,1)S(1)}, bf16[2,128,256]{2,1,0:T(8,128)(2,1)S(1)}, u32[]{:S(2)}, u32[]{:S(2)}) collective-permute-start(bf16[2,128,256]{2,1,0:T(8,128)(2,1)S(1)} %collective-permute-done.own1), channel_id=1, source_target_pairs={{0,128},{1,385},{128,256},{129,1},{256,384},{257,129},{384,0},{385... | collective-permute-start | bytes 393224 | tf_op jit(solution)/shard_map/ppermute | solution.py:32
  57.9 3.4 %collective-permute-start.3 = (bf16[4,128,256]{2,1,0:T(8,128)(2,1)S(1)}, bf16[4,128,256]{2,1,0:T(8,128)(2,1)S(1)}, u32[]{:S(2)}, u32[]{:S(2)}) collective-permute-start(bf16[4,128,256]{2,1,0:T(8,128)(2,1)S(1)} %pad_maximum_fusion), channel_id=1, source_target_pairs={{0,1},{1,0},{2,3},{3,2},{4,5},{5,4},{6,7},{7,6},{8,9},{9,8},{10,11... | collective-permute-start | bytes 786440 | tf_op jit(solution)/shard_map/ppermute | solution.py:23
  62.5 5.8 %copy-start.1 = (f32[16,1,128,128]{3,2,1,0:T(8,128)S(1)}, f32[16,1,128,128]{3,2,1,0:T(8,128)}, u32[]{:S(2)}) copy-start(f32[16,1,128,128]{3,2,1,0:T(8,128)} %param.23) | copy-start | bytes 3145732
  62.5 13.4 %all-to-all-start.3 = ((bf16[4,136,512]{2,1,0:T(8,128)(2,1)}), bf16[4,136,512]{2,1,0:T(8,128)(2,1)S(1)}, u32[]{:S(2)}, u32[]{:S(2)}) async-start(bf16[4,136,512]{2,1,0:T(8,128)(2,1)} %shard_map.177), calls=%async_computation.3 | async-start | bytes 1114112 | tf_op jit(solution)/shard_map/all_to_all | solution.py:36
  66.3 3.4 %collective-permute-start.4 = (bf16[4,128,256]{2,1,0:T(8,128)(2,1)S(1)}, bf16[4,128,256]{2,1,0:T(8,128)(2,1)S(1)}, u32[]{:S(2)}, u32[]{:S(2)}) collective-permute-start(bf16[4,128,256]{2,1,0:T(8,128)(2,1)S(1)} %pad_maximum_fusion.1), channel_id=1, source_target_pairs={{0,1},{1,0},{2,3},{3,2},{4,5},{5,4},{6,7},{7,6},{8,9},{9,8},{10,11... | collective-permute-start | bytes 786440 | tf_op jit(solution)/shard_map/ppermute | solution.py:23
